TPU v7x, 768 devices: a whole 4x8x12 slice. The times are simulated.
768 devices in a mesh: fs: 96 (over z, y), tp: 8 (over x, core).
Axes of the slice: x: 4, y: 8, z: 12, core: 2. Of those that a mesh axis runs over, the one named last changes fastest.
Arguments:
- inputs: bfloat16 [49152, 2304], P('fs'), may hold values from -6 to 6
- value_cot: bfloat16 [49152, 4096], P('fs', 'tp'), may hold values from -0.026977539 to 0.026977539
- retained: bfloat16 [49152, 4096], P('fs', 'tp'), may hold values from -6 to 6
- output_cot: bfloat16 [49152, 2304], P('fs'), may hold values from -0.026977539 to 0.026977539
- proj_value: bfloat16 [2304, 192], P('fs'), may hold values from -0.125 to 0.125
- proj_output: bfloat16 [2304, 192], P('fs'), may hold values from -0.125 to 0.125
- w_value: float32 [2304, 4096], P('fs', 'tp'), may hold values from -6 to 6
- w_output: float32 [4096, 2304], P('tp', 'fs'), may hold values from -6 to 6
- first_value: float32 [192, 4096], P('fs', 'tp'), may hold values from -106 to 106
- second_value: float32 [192, 4096], P('fs', 'tp'), may hold values from 0.25 to 4
- first_output: float32 [192, 4096], P('fs', 'tp'), may hold values from -106 to 106
- second_output: float32 [192, 4096], P('fs', 'tp'), may hold values from 0.25 to 4
Outputs:
- step_value: float32 [2304, 4096], P('fs', 'tp')
- step_output: float32 [4096, 2304], P('tp', 'fs')
- copy_value: bfloat16 [2304, 4096], P(None, 'tp')
- copy_output: bfloat16 [4096, 2304], P('tp')
- new_first_value: float32 [192, 4096], P('fs', 'tp')
- new_second_value: float32 [192, 4096], P('fs', 'tp')
- new_first_output: float32 [192, 4096], P('fs', 'tp')
- new_second_output: float32 [192, 4096], P('fs', 'tp')
All inputs are finite; a program needn't handle non-finite values.
Results may differ from a plain program's by a relative error of at most 0.0034.
Values may be sent and summed in bfloat16 or wider, within the bound.
No kernel may reach another device: no remote copies, remote signals or barrier semaphores. Data moves between devices by JAX's collectives and lax.ppermute only.
A program may use at most 64 MiB of HBM per device.

v0:
```python
import jax
import jax.numpy as jnp
from jax import lax
from jax.sharding import Mesh
from jax.sharding import PartitionSpec as P

RANK = 192
HV = 4096
FS = ("fs_0", "fs_1")


beta_one = 0.8
beta_two = 0.9
moment_eps = 1e-08
norm_eps = 1e-06


def side_by_side(arrays, axis, dim, along):
    both = jnp.concatenate(arrays, axis=along)
    out, at, outs = (lax.all_gather(both, axis, axis=dim, tiled=True), 0, [])
    for a in arrays:
        outs.append(lax.slice_in_dim(out, at, at + a.shape[along], axis=along))
        at += a.shape[along]
    return tuple(outs)


def rows_first(arrays, axis, dims):
    turned = [jnp.moveaxis(a, dim, 0) for a, dim in zip(arrays, dims)]
    widths = [t[0].size for t in turned]
    both = jnp.concatenate([t.reshape(-1, w) for t, w in zip(turned, widths)], axis=1)
    out = lax.all_gather(both, axis, axis=0, tiled=True)
    pieces = jnp.split(out, [sum(widths[:k]) for k in range(1, len(widths))], axis=1)
    return tuple(
        (
            jnp.moveaxis(b.reshape(-1, *t.shape[1:]), 0, dim)
            for b, t, dim in zip(pieces, turned, dims)
        )
    )


def reduced_to_own(pieces, axes, turns):
    inside = pieces.shape[1:]
    pieces = pieces.reshape(*(lax.axis_size(a) for a in axes), *inside)
    pieces = jnp.moveaxis(pieces, turns, range(len(axes))).reshape(-1, *inside)
    for k in turns:
        pieces = lax.psum_scatter(pieces, axes[k], scatter_dimension=0, tiled=True)
    return pieces[0]


def split_up(value, dim, length):
    before, after = (value.shape[:dim], value.shape[dim + 1 :])
    return jnp.moveaxis(value.reshape(*before, length, -1, *after), dim, 0)


def scatter_axes(value, axes, turns, dim):
    length = lax.axis_size(axes)
    return reduced_to_own(split_up(value, dim, length), axes, turns)


def copy_for_each(value, axis):
    copies = jnp.broadcast_to(value, (lax.axis_size(axis), *value.shape))
    return lax.all_to_all(copies, axis, split_axis=0, concat_axis=0, tiled=True)


def over_copies(value, axis):
    return copy_for_each(value, axis).sum(axis=0)


def in_one(arrays, axis):
    ends = [0]
    for a in arrays:
        ends.append(ends[-1] + a.size)
    total = over_copies(jnp.concatenate([a.ravel() for a in arrays]), axis)
    return tuple((total[b:e].reshape(a.shape) for a, b, e in zip(arrays, ends, ends[1:])))


def project_rows(inputs, output_cot, pieces):
    return (
        jnp.dot(inputs, pieces[0], preferred_element_type=jnp.float32),
        jnp.dot(output_cot, pieces[1], preferred_element_type=jnp.float32),
    )


def contract_tokens(left, right):
    return lax.dot_general(
        left, right, (((0,), (0,)), ((), ())), preferred_element_type=jnp.float32
    )


def adapt(first, second, grad):
    new_first = beta_one * first + (1.0 - beta_one) * grad
    new_second = beta_two * second + (1.0 - beta_two) * grad * grad
    direction = (new_first / (jnp.sqrt(new_second) + moment_eps)).astype(jnp.bfloat16)
    return (new_first, new_second, direction)


def squares(direction):
    return jnp.sum(jnp.square(direction.astype(jnp.float32)))


def expand(proj_value, proj_output, update_v, update_o, pieces):
    update_v = jnp.dot(proj_value, pieces[0], preferred_element_type=jnp.float32)
    update_o = lax.dot_general(
        pieces[1], proj_output, (((0,), (1,)), ((), ())), preferred_element_type=jnp.float32
    )
    return (update_v, update_o)


def per_device(
    inputs,
    value_cot,
    retained,
    output_cot,
    proj_value,
    proj_output,
    w_value,
    w_output,
    first_value,
    second_value,
    first_output,
    second_output,
):
    block_width = proj_value.shape[1] // lax.axis_size("tp")
    offset = lax.axis_index("tp") * block_width
    own_value = lax.dynamic_slice_in_dim(proj_value, offset, block_width, 1)
    own_output = lax.dynamic_slice_in_dim(proj_output, offset, block_width, 1)
    folded = project_rows(inputs, output_cot, side_by_side((own_value, own_output), FS, 0, 1))
    narrow = (folded[0].astype(jnp.bfloat16), folded[1].astype(jnp.bfloat16))
    x_proj, o_proj = rows_first((narrow[0], narrow[1]), "tp", (1, 1))
    summed = scatter_axes(
        jnp.concatenate(
            [contract_tokens(x_proj, value_cot), contract_tokens(o_proj, retained)], axis=1
        ),
        FS,
        (1, 0),
        0,
    )
    columns = value_cot.shape[1]
    first_v, second_v, dir_value = adapt(first_value, second_value, summed[:, :columns])
    first_o, second_o, dir_output = adapt(first_output, second_output, summed[:, columns:])
    zero_v = jnp.zeros((proj_value.shape[0], columns), jnp.float32)
    zero_o = jnp.zeros((columns, proj_output.shape[0]), jnp.float32)
    start_state = (zero_v, zero_o, jnp.zeros((), jnp.float32), jnp.zeros((), jnp.float32))
    pieces = side_by_side((dir_value, dir_output), FS, 0, 1)
    update_v, update_o = expand(proj_value, proj_output, start_state[0], start_state[1], pieces)
    totals = in_one((squares(pieces[0]), squares(pieces[1])), "tp")
    scale_value = lax.rsqrt(totals[0] / (RANK * HV) + norm_eps)
    scale_output = lax.rsqrt(totals[1] / (RANK * HV) + norm_eps)
    step_value = update_v * scale_value
    step_output = update_o * scale_output
    fresh = (
        (w_value + step_value).astype(jnp.bfloat16),
        (w_output + step_output).astype(jnp.bfloat16),
    )
    copy_value, copy_output = rows_first((fresh[0], fresh[1]), FS, (0, 1))
    return (step_value, step_output, copy_value, copy_output, first_v, second_v, first_o, second_o)


def solution(mesh):
    split = Mesh(mesh.devices.reshape(12, 8, mesh.shape["tp"]), ("fs_0", "fs_1", "tp"))
    return jax.shard_map(
        per_device,
        mesh=split,
        in_specs=(
            P(FS, None),
            P(FS, "tp"),
            P(FS, "tp"),
            P(FS, None),
            P(FS, None),
            P(FS, None),
            P(FS, "tp"),
            P("tp", FS),
            P(FS, "tp"),
            P(FS, "tp"),
            P(FS, "tp"),
            P(FS, "tp"),
        ),
        out_specs=(
            P(FS, "tp"),
            P("tp", FS),
            P(None, "tp"),
            P("tp", None),
            P(FS, "tp"),
            P(FS, "tp"),
            P(FS, "tp"),
            P(FS, "tp"),
        ),
        check_vma=False,
    )
```

profile of v0, /device:TPU:6, one launch (start us, length us, event | category | flops | bytes accessed | tf_op | source)
XLA Modules:
  0.0 528.0 jit_solution(12694136843098188866)
XLA Ops:
  7.2 0.0 copy-start
  7.2 0.0 all-reduce.5.cloned.1.call-start
  7.2 0.0 copy-start.1
  7.2 0.9 constant_dynamic-slice_fusion.1
  8.2 0.1 pad_maximum_fusion.3
  8.3 83.9 %all_gather.12 = bf16[2304,48]{1,0:T(8,128)(2,1)S(1)} all-gather(bf16[24,48]{1,0:T(8,128)(2,1)S(1)} %pad_maximum_fusion.3), channel_id=1, replica_groups=mesh['fs_0'=12,'fs_1'=8,'tp'=8] {'fs_0','fs_1'}, dimensions={0}, use_global_device_ids=true | all-gather | bytes 223488 | tf_op jit(solution)/shard_map/all_gather | solution.py:20
  92.1 1.1 convolution_convert_fusion
  93.2 0.0 copy-start.2
  93.3 0.0 copy-start.3
  93.3 0.7 convolution_convert_fusion.1
  94.0 13.0 %all_gather.13 = bf16[192,1024]{1,0:T(8,128)(2,1)S(1)} all-gather(bf16[24,1024]{1,0:T(8,128)(2,1)S(1)} %pad_maximum_fusion.1), channel_id=1, replica_groups=mesh['fs_0'=12,'fs_1'=8,'tp'=8] {'tp'}, dimensions={0}, use_global_device_ids=true | all-gather | bytes 442368 | tf_op jit(solution)/shard_map/all_gather | solution.py:31
  107.0 0.0 copy-done.2
  107.0 0.3 fusion.3
  107.3 0.0 copy-done.3
  107.3 0.3 fusion.5
  107.5 0.1 pad_maximum_fusion
  107.6 0.0 copy-start.8
  107.6 0.0 copy-start.9
  107.6 0.0 copy-start.10
  107.6 0.0 copy-start.11
  107.7 1.3 reshape_reshape.3
  109.0 2.1 copy.26
  111.1 0.0 all-reduce.5.cloned.1.call-update
  111.2 0.0 all-reduce.7.cloned.1.call-start
  111.2 1.3 dynamic-slice
  113.1 78.6 %all-reduce.5.cloned.1.call-done = f32[96,2,1024]{2,1,0:T(2,128)} async-done(((f32[96,2,1024]{2,1,0:T(2,128)}), f32[96,2,1024]{2,1,0:T(2,128)}) %all-reduce.5.cloned.1.call-update) | async-done | bytes 786448
  191.7 1.5 constant_dynamic-slice_fusion
  193.3 0.0 all-reduce.7.cloned.1.call-update
  193.3 0.0 all-gather.3.cloned.1.call-start
  193.3 1.3 dynamic-slice.2
  194.6 111.4 %all-reduce.7.cloned.1.call-done = f32[12,2,1024]{2,1,0:T(2,128)} async-done(((f32[12,2,1024]{2,1,0:T(2,128)}), f32[12,2,1024]{2,1,0:T(2,128)}) %all-reduce.7.cloned.1.call-update) | async-done | bytes 98320
  306.0 1.3 dynamic-slice_bitcast_fusion
  307.3 0.0 copy-done.9
  307.3 0.6 fusion.12
  308.0 68.5 %all-gather = bf16[96,2,1024]{2,1,0:T(2,128)(2,1)S(1)} all-gather(bf16[1,2,1024]{2,1,0:T(2,128)(2,1)S(1)} %maximum_bitcast_fusion), channel_id=1, replica_groups=mesh['fs_0'=12,'fs_1'=8,'tp'=8] {'fs_0','fs_1'}, dimensions={0}, use_global_device_ids=true | all-gather | bytes 397312 | tf_op jit(solution)/shard_map/all_gather | solution.py:20
  376.5 0.1 reshape.45
  376.6 0.7 multiply_reduce_fusion.1
  377.4 1.4 pad_maximum_fusion.4
  378.7 7.8 %all_to_all.6 = f32[8,1,2]{2,1,0:T(1,128)S(1)} all-to-all(f32[8,1,2]{2,1,0:T(1,128)S(1)} %broadcast_in_dim.3), channel_id=1, replica_groups=mesh['fs_0'=12,'fs_1'=8,'tp'=8] {'tp'}, dimensions={0} | all-to-all | bytes 128 | tf_op jit(solution)/shard_map/all_to_all | solution.py:62
  386.6 0.6 fusion.16
  388.6 0.1 convolution_multiply_fusion
  388.7 0.0 copy-done.6
  388.7 0.8 add_convert_fusion.1
  389.5 0.6 pad_maximum_fusion.2
  390.1 0.0 all-gather.3.cloned.1.call-update
  390.2 122.2 %all-gather.3.cloned.1.call-done = bf16[2304,1024]{1,0:T(8,128)(2,1)} async-done(((bf16[24,1024]{1,0:T(8,128)(2,1)}), bf16[2304,1024]{1,0:T(8,128)(2,1)}) %all-gather.3.cloned.1.call-update) | async-done | bytes 4718608 | tf_op jit(solution)/shard_map/all_gather | solution.py:31
  512.4 4.9 slice_bitcast_fusion
  517.2 4.3 copy.28
  (19 shorter events, 0.1 us)
Async XLA Ops:
  7.2 85.0 %copy-start = (bf16[512,2304]{1,0:T(8,128)(2,1)S(1)}, bf16[512,2304]{1,0:T(8,128)(2,1)}, u32[]{:S(2)}) copy-start(bf16[512,2304]{1,0:T(8,128)(2,1)} %param.15) | copy-start | bytes 7077892
  7.2 184.5 %all-reduce.5.cloned.1.call-start = ((), (), s32[]{:S(2)}) async-start(), calls=%async_computation.2 | async-start | bytes 1572864
  7.2 86.0 %copy-start.1 = (bf16[512,2304]{1,0:T(8,128)(2,1)S(1)}, bf16[512,2304]{1,0:T(8,128)(2,1)}, u32[]{:S(2)}) copy-start(bf16[512,2304]{1,0:T(8,128)(2,1)} %param.12) | copy-start | bytes 7077892
  93.2 13.8 %copy-start.2 = (bf16[512,512]{1,0:T(8,128)(2,1)S(1)}, bf16[512,512]{1,0:T(8,128)(2,1)}, u32[]{:S(2)}) copy-start(bf16[512,512]{1,0:T(8,128)(2,1)} %param.14) | copy-start | bytes 1572868
  93.3 14.0 %copy-start.3 = (bf16[512,512]{1,0:T(8,128)(2,1)S(1)}, bf16[512,512]{1,0:T(8,128)(2,1)}, u32[]{:S(2)}) copy-start(bf16[512,512]{1,0:T(8,128)(2,1)} %param.13) | copy-start | bytes 1572868
  107.6 199.7 %copy-start.8 = (f32[2,512]{1,0:T(2,128)S(1)}, f32[2,512]{1,0:T(2,128)}, u32[]{:S(2)}) copy-start(f32[2,512]{1,0:T(2,128)} %param.21) | copy-start | bytes 12292
  107.6 199.7 %copy-start.9 = (f32[2,512]{1,0:T(2,128)S(1)}, f32[2,512]{1,0:T(2,128)}, u32[]{:S(2)}) copy-start(f32[2,512]{1,0:T(2,128)} %param.20) | copy-start | bytes 12292
  107.6 199.7 %copy-start.10 = (f32[2,512]{1,0:T(2,128)S(1)}, f32[2,512]{1,0:T(2,128)}, u32[]{:S(2)}) copy-start(f32[2,512]{1,0:T(2,128)} %param.23) | copy-start | bytes 12292
  107.6 199.7 %copy-start.11 = (f32[2,512]{1,0:T(2,128)S(1)}, f32[2,512]{1,0:T(2,128)}, u32[]{:S(2)}) copy-start(f32[2,512]{1,0:T(2,128)} %param.22) | copy-start | bytes 12292
  109.0 279.6 %copy-start.12 = (bf16[24,192]{1,0:T(8,128)(2,1)S(1)}, bf16[24,192]{1,0:T(8,128)(2,1)}, u32[]{:S(2)}) copy-start(bf16[24,192]{1,0:T(8,128)(2,1)} %param.17) | copy-start | bytes 27652
  109.0 279.7 %copy-start.6 = (f32[24,512]{1,0:T(8,128)S(1)}, f32[24,512]{1,0:T(8,128)}, u32[]{:S(2)}) copy-start(f32[24,512]{1,0:T(8,128)} %param.18) | copy-start | bytes 147460
  109.0 279.7 %copy-start.7 = (bf16[24,192]{1,0:T(8,128)(2,1)S(1)}, bf16[24,192]{1,0:T(8,128)(2,1)}, u32[]{:S(2)}) copy-start(bf16[24,192]{1,0:T(8,128)(2,1)} %param.16) | copy-start | bytes 27652
  109.0 280.5 %copy-start.4 = (f32[512,24]{0,1:T(8,128)S(1)}, f32[512,24]{0,1:T(8,128)}, u32[]{:S(2)}) copy-start(f32[512,24]{0,1:T(8,128)} %param.19) | copy-start | bytes 147460
  111.2 194.8 %all-reduce.7.cloned.1.call-start = ((), (), s32[]{:S(2)}) async-start(), calls=%async_computation.3 | async-start | bytes 196608
  193.3 319.1 %all-gather.3.cloned.1.call-start = ((), (), s32[]{:S(2)}) async-start(), calls=%async_computation.1 | async-start | bytes 4767744 | tf_op jit(solution)/shard_map/all_gather | solution.py:31
  388.7 128.5 %copy-start.5 = (f32[512,24]{0,1:T(8,128)}, f32[512,24]{0,1:T(8,128)S(1)}, u32[]{:S(2)}) copy-start(f32[512,24]{0,1:T(8,128)S(1)} %convolution_multiply_fusion) | copy-start | bytes 147460
Sparse Core Ops, SparseCore 0:
  111.3 80.3 all-reduce.4
  194.6 111.3 all-reduce.6
  390.3 122.0 all-gather.2
where the time goes:
time: 529 us; the launch traced here: 528 us
  waiting for transfers between devices  312 us (59%)
  blocking collectives  173 us (33%)
  local copies, waits for them, and re-layouts  19.8 us (4%)
  between operations  16 us (3%)
    unnamed x5, waiting for transfers between devices  190 us
    all_gather x2, blocking collectives, side_by_side(): out, at, outs = (lax.all_gather(both, axis, axis=dim, tiled=True), 0, [])  152 us
    all_gather x1, waiting for transfers between devices, rows_first(): out = lax.all_gather(both, axis, axis=0, tiled=True)  122 us
    all_gather x1, blocking collectives, rows_first(): out = lax.all_gather(both, axis, axis=0, tiled=True)  13 us
  transfers between devices with their start and end apart: 3, of which 3 were waited for; matrix products, arithmetic and copies ran while one was open for 0% of the time, Pallas kernels for 0%

commit v1 on v0

v1 whole, which is shorter than its diff:
```python
import jax
import jax.numpy as jnp
from jax import lax
from jax.sharding import Mesh
from jax.sharding import PartitionSpec as P

RANK = 192
HV = 4096
FS = ("fs_0", "fs_1")


beta_one = 0.8
beta_two = 0.9
moment_eps = 1e-08
norm_eps = 1e-06


def exchange(pieces, axis):
    return lax.all_to_all(pieces, axis, split_axis=0, concat_axis=0, tiled=True)


def spread(value, axis):
    return exchange(jnp.broadcast_to(value, (lax.axis_size(axis), *value.shape)), axis)


def contract(left, right, dims):
    return lax.dot_general(left, right, (dims, ((), ())), preferred_element_type=jnp.float32)


def adapt(first, second, grad):
    new_first = beta_one * first + (1.0 - beta_one) * grad
    new_second = beta_two * second + (1.0 - beta_two) * grad * grad
    direction = (new_first / (jnp.sqrt(new_second) + moment_eps)).astype(jnp.bfloat16)
    return (new_first, new_second, direction)


def squares(direction):
    return jnp.sum(jnp.square(direction.astype(jnp.float32)))


def per_device(
    inputs,
    value_cot,
    retained,
    output_cot,
    proj_value,
    proj_output,
    w_value,
    w_output,
    first_value,
    second_value,
    first_output,
    second_output,
):
    bf16 = jnp.bfloat16
    rank = proj_value.shape[1]
    columns = value_cot.shape[1]
    early = jnp.concatenate(
        [w_value.astype(bf16), w_output.T.astype(bf16), proj_value, proj_output], axis=1
    )
    early = lax.all_gather(early, FS, axis=0, tiled=True)
    wide_value = early[:, :columns]
    wide_output = early[:, columns : 2 * columns]
    full_value = early[:, 2 * columns : 2 * columns + rank]
    full_output = early[:, 2 * columns + rank :]

    width = rank // lax.axis_size("tp")
    offset = lax.axis_index("tp") * width
    own = jnp.concatenate(
        [
            lax.dynamic_slice_in_dim(proj_value, offset, width, 1),
            lax.dynamic_slice_in_dim(proj_output, offset, width, 1),
        ],
        axis=1,
    )
    rows = spread(own, "fs_0")
    rows = spread(rows.reshape(-1, 2 * width), "fs_1")
    rows = rows.reshape(lax.axis_size("fs_1"), lax.axis_size("fs_0"), -1, 2 * width)
    rows = jnp.swapaxes(rows, 0, 1).reshape(-1, 2 * width)
    narrow = jnp.concatenate(
        [
            contract(rows[:, :width], inputs, ((0,), (1,))),
            contract(rows[:, width:], output_cot, ((0,), (1,))),
        ],
        axis=0,
    ).astype(bf16)
    projected = spread(narrow, "tp")
    x_proj = projected[:, :width].reshape(rank, -1)
    o_proj = projected[:, width:].reshape(rank, -1)

    partial = jnp.concatenate(
        [contract(x_proj, value_cot, ((1,), (0,))), contract(o_proj, retained, ((1,), (0,)))],
        axis=1,
    ).astype(bf16)
    pieces = exchange(partial.reshape(lax.axis_size(FS), -1, 2 * columns), FS)
    summed = pieces.astype(jnp.float32).sum(axis=0)
    first_v, second_v, dir_value = adapt(first_value, second_value, summed[:, :columns])
    first_o, second_o, dir_output = adapt(first_output, second_output, summed[:, columns:])

    dirs = spread(jnp.concatenate([dir_value, dir_output], axis=1), FS).reshape(rank, -1)
    dir_value, dir_output = (dirs[:, :columns], dirs[:, columns:])
    sums = jnp.stack([squares(dir_value), squares(dir_output)])
    totals = spread(sums[None], "tp").sum(axis=(0, 1))
    scale_value = lax.rsqrt(totals[0] / (RANK * HV) + norm_eps)
    scale_output = lax.rsqrt(totals[1] / (RANK * HV) + norm_eps)

    step_value = contract(proj_value, dir_value, ((1,), (0,))) * scale_value
    step_output = contract(dir_output, proj_output, ((0,), (1,))) * scale_output
    copy_value = contract(full_value, dir_value, ((1,), (0,))) * scale_value
    copy_value = (wide_value.astype(jnp.float32) + copy_value).astype(bf16)
    copy_output = contract(dir_output, full_output, ((0,), (1,))) * scale_output
    copy_output = (wide_output.T.astype(jnp.float32) + copy_output).astype(bf16)
    return (step_value, step_output, copy_value, copy_output, first_v, second_v, first_o, second_o)


def solution(mesh):
    split = Mesh(mesh.devices.reshape(12, 8, mesh.shape["tp"]), ("fs_0", "fs_1", "tp"))
    return jax.shard_map(
        per_device,
        mesh=split,
        in_specs=(
            P(FS, None),
            P(FS, "tp"),
            P(FS, "tp"),
            P(FS, None),
            P(FS, None),
            P(FS, None),
            P(FS, "tp"),
            P("tp", FS),
            P(FS, "tp"),
            P(FS, "tp"),
            P(FS, "tp"),
            P(FS, "tp"),
        ),
        out_specs=(
            P(FS, "tp"),
            P("tp", FS),
            P(None, "tp"),
            P("tp", None),
            P(FS, "tp"),
            P(FS, "tp"),
            P(FS, "tp"),
            P(FS, "tp"),
        ),
        check_vma=False,
    )
```

time: 529 us -> 180 us (0.34)
  waiting for transfers between devices: 312 us -> 10.8 us
  blocking collectives: 173 us -> 124 us
  local copies, waits for them, and re-layouts: 19.8 us -> 9.4 us
  matrix products: 3.25 us -> 13.6 us
    unnamed x5 -> x1, waiting for transfers between devices: 190 us -> 0.02 us
    all_gather x3 -> x0, blocking collectives: 165 us -> none  [the longest x2 152 us: side_by_side(): out, at, outs = (lax.all_gather(both, axis, axis=dim, tiled=True), 0, [])]
    all_to_all x1 -> x6, blocking collectives: 7.81 us -> 124 us  [exchange(): return lax.all_to_all(pieces, axis, split_axis=0, concat_axis=0, tiled=True)]
    all_gather x1, waiting for transfers between devices: 122 us -> 10.8 us  [per_device(): early = lax.all_gather(early, FS, axis=0, tiled=True)]
    dot_general x6 -> x8, matrix products: 3.25 us -> 13.6 us  [contract(): lax.dot_general(left, right, (dims, ((), ())), preferred_element_type=jnp...]
    transpose x2 -> x1, local copies, waits for them, and re-layouts: 6.98 us -> 0.07 us  [per_device(): rows = jnp.swapaxes(rows, 0, 1).reshape(-1, 2 * width)]
  transfers between devices with their start and end apart: 3 -> 1, of which waited for: 3 -> 1; matrix products, arithmetic and copies ran while one was open for 0% -> 6% of each run, Pallas kernels for 0% -> 0%
where the time goes in v1:
time: 180 us; the launch traced here: 179 us
  blocking collectives  124 us (69%)
  between operations  15.6 us (9%)
  matrix products  13.6 us (8%)
  waiting for transfers between devices  10.8 us (6%)
  local copies, waits for them, and re-layouts  9.4 us (5%)
  other arithmetic  5 us (3%)
    all_to_all x6, blocking collectives, exchange(): return lax.all_to_all(pieces, axis, split_axis=0, concat_axis=0, tiled=True)  124 us
    dot_general x8, matrix products, contract(): lax.dot_general(left, right, (dims, ((), ())), preferred_element_type=jnp...  13.6 us
    all_gather x1, waiting for transfers between devices, per_device(): early = lax.all_gather(early, FS, axis=0, tiled=True)  10.8 us
    unnamed x21, local copies, waits for them, and re-layouts  5.06 us
  transfers between devices with their start and end apart: 1, of which 1 were waited for; matrix products, arithmetic and copies ran while one was open for 6% of the time, Pallas kernels for 0%

profile of v1, /device:TPU:6, one launch (start us, length us, event | category | flops | bytes accessed | tf_op | source)
XLA Modules:
  0.0 179.0 jit_solution(12664956287250521477)
XLA Ops:
  7.2 0.0 copy-start
  7.2 0.0 all-gather.2.cloned.1.call-start
  7.2 1.0 convert_bitcast_fusion
  8.2 0.8 convert_element_type.47
  9.0 1.4 concatenate.22
  10.4 0.0 all-gather.2.cloned.1.call-update
  10.5 0.8 constant_dynamic-slice_fusion
  11.3 0.1 pad_maximum_fusion.2
  11.4 0.1 reshape.53
  11.5 25.5 %all_to_all.30 = bf16[12,2,576]{2,1,0:T(2,128)(2,1)S(1)} all-to-all(bf16[12,2,576]{2,1,0:T(2,128)(2,1)S(1)} %reshape.53), channel_id=1, replica_groups=mesh['fs_0'=12,'fs_1'=8,'tp'=8] {'fs_0'}, dimensions={0} | all-to-all | bytes 55296 | tf_op jit(solution)/shard_map/all_to_all | solution.py:19
  37.0 0.1 reshape.54
  37.1 0.1 copy.55
  37.3 18.6 %all_to_all.31 = bf16[8,288,48]{1,2,0:T(8,128)(2,1)S(1)} all-to-all(bf16[8,288,48]{1,2,0:T(8,128)(2,1)S(1)} %broadcast_in_dim.17), channel_id=1, replica_groups=mesh['fs_0'=12,'fs_1'=8,'tp'=8] {'fs_1'}, dimensions={0} | all-to-all | bytes 442368 | tf_op jit(solution)/shard_map/all_to_all | solution.py:19
  55.9 0.3 copy.56
  56.2 0.1 copy.57
  56.3 0.0 copy-done
  56.3 1.1 convolution_convert_fusion.2
  57.4 0.5 copy-done.1
  57.8 0.7 convolution_convert_fusion.3
  58.6 11.4 %all_to_all.32 = bf16[8,48,512]{2,1,0:T(8,128)(2,1)S(1)} all-to-all(bf16[8,48,512]{2,1,0:T(8,128)(2,1)S(1)} %broadcast_in_dim.18), channel_id=1, replica_groups=mesh['fs_0'=12,'fs_1'=8,'tp'=8] {'tp'}, dimensions={0} | all-to-all | bytes 786432 | tf_op jit(solution)/shard_map/all_to_all | solution.py:19
  70.1 0.1 dot_general.32
  70.2 0.1 dot_general.30
  70.3 0.0 copy-start.5
  70.3 0.0 copy-start.6
  70.3 0.0 copy-start.7
  70.3 0.0 copy-start.8
  70.3 0.3 convolution_convert_fusion
  70.6 1.3 convolution_convert_fusion.1
  71.9 0.0 copy-start.3
  72.0 0.0 copy-start.4
  72.0 0.4 copy.60
  72.4 29.4 %all_to_all.33 = bf16[96,2,1024]{2,1,0:T(2,128)(2,1)S(1)} all-to-all(bf16[96,2,1024]{2,1,0:T(2,128)(2,1)S(1)} %copy.60), channel_id=1, replica_groups=mesh['fs_0'=12,'fs_1'=8,'tp'=8] {'fs_0','fs_1'}, dimensions={0} | all-to-all | bytes 786432 | tf_op jit(solution)/shard_map/all_to_all | solution.py:19
  101.8 0.4 convert_reduce_fusion
  102.2 0.6 fusion.19
  102.8 0.2 broadcast_in_dim.19
  103.0 31.6 %all_to_all.34 = bf16[96,2,1024]{2,1,0:T(2,128)(2,1)S(1)} all-to-all(bf16[96,2,1024]{2,1,0:T(2,128)(2,1)S(1)} %broadcast_in_dim.19), channel_id=1, replica_groups=mesh['fs_0'=12,'fs_1'=8,'tp'=8] {'fs_0','fs_1'}, dimensions={0} | all-to-all | bytes 786432 | tf_op jit(solution)/shard_map/all_to_all | solution.py:19
  134.7 0.1 reshape.50
  134.8 0.7 multiply_reduce_fusion.1
  135.6 1.4 pad_maximum_fusion.4
  136.9 7.9 %all_to_all.35 = f32[8,1,2]{2,1,0:T(1,128)S(1)} all-to-all(f32[8,1,2]{2,1,0:T(1,128)S(1)} %broadcast_in_dim.20), channel_id=1, replica_groups=mesh['fs_0'=12,'fs_1'=8,'tp'=8] {'tp'}, dimensions={0} | all-to-all | bytes 128 | tf_op jit(solution)/shard_map/all_to_all | solution.py:19
  144.9 0.6 fusion.24
  146.8 0.0 copy-done.3
  146.8 0.8 convolution_multiply_fusion.2
  147.6 0.8 fusion.6
  148.4 10.8 %all-gather.2.cloned.1.call-done = bf16[2304,1408]{1,0:T(8,128)(2,1)} async-done(((bf16[24,1408]{1,0:T(8,128)(2,1)}), bf16[2304,1408]{1,0:T(8,128)(2,1)}) %all-gather.2.cloned.1.call-update) | async-done | bytes 6488080 | tf_op jit(solution)/shard_map/all_gather | solution.py:61
  159.2 4.4 %fusion.3 = bf16[512,2304]{0,1:T(8,128)(2,1)} fusion(bf16[2304,1408]{1,0:T(8,128)(2,1)} %all-gather.2.cloned.1.call-done, f32[]{:T(128)} %bitcast.10, bf16[192,1024]{1,0:T(8,128)(2,1)S(1)} %reshape.50), kind=kOutput, calls=%fused_computation.5 | convolution fusion | flops 457703424 | bytes 6095360 | tf_op jit(solution)/shard_map/dot_general | solution.py:27
  163.6 4.3 %copy.63 = bf16[512,2304]{1,0:T(8,128)(2,1)} copy(bf16[512,2304]{0,1:T(8,128)(2,1)} %fusion.3) | data formatting | bytes 4718592
  167.9 4.2 %fusion.2 = bf16[2304,512]{1,0:T(8,128)(2,1)} fusion(bf16[2304,1408]{1,0:T(8,128)(2,1)} %all-gather.2.cloned.1.call-done, f32[]{:T(128)} %bitcast.8, bf16[192,1024]{1,0:T(8,128)(2,1)S(1)} %reshape.50), kind=kOutput, calls=%fused_computation.4 | convolution fusion | flops 457703424 | bytes 6095360 | tf_op jit(solution)/shard_map/dot_general | solution.py:27
  (17 shorter events, 0.2 us)
Async XLA Ops:
  7.2 49.1 %copy-start = (bf16[512,2304]{1,0:T(8,128)(2,1)S(1)}, bf16[512,2304]{1,0:T(8,128)(2,1)}, u32[]{:S(2)}) copy-start(bf16[512,2304]{1,0:T(8,128)(2,1)} %param.15) | copy-start | bytes 7077892
  7.2 152.0 %all-gather.2.cloned.1.call-start = ((), (), s32[]{:S(2)}) async-start(), calls=%async_computation.6 | async-start | bytes 6555648 | tf_op jit(solution)/shard_map/all_gather | solution.py:61
  56.2 1.7 copy-start.1
  57.8 12.4 %copy-start.2 = (bf16[512,512]{1,0:T(8,128)(2,1)S(1)}, bf16[512,512]{1,0:T(8,128)(2,1)}, u32[]{:S(2)}) copy-start(bf16[512,512]{1,0:T(8,128)(2,1)} %param.14) | copy-start | bytes 1572868
  70.3 31.9 %copy-start.5 = (f32[2,512]{1,0:T(2,128)S(1)}, f32[2,512]{1,0:T(2,128)}, u32[]{:S(2)}) copy-start(f32[2,512]{1,0:T(2,128)} %param.21) | copy-start | bytes 12292
  70.3 31.9 %copy-start.6 = (f32[2,512]{1,0:T(2,128)S(1)}, f32[2,512]{1,0:T(2,128)}, u32[]{:S(2)}) copy-start(f32[2,512]{1,0:T(2,128)} %param.20) | copy-start | bytes 12292
  70.3 31.9 %copy-start.7 = (f32[2,512]{1,0:T(2,128)S(1)}, f32[2,512]{1,0:T(2,128)}, u32[]{:S(2)}) copy-start(f32[2,512]{1,0:T(2,128)} %param.23) | copy-start | bytes 12292
  70.3 31.9 %copy-start.8 = (f32[2,512]{1,0:T(2,128)S(1)}, f32[2,512]{1,0:T(2,128)}, u32[]{:S(2)}) copy-start(f32[2,512]{1,0:T(2,128)} %param.22) | copy-start | bytes 12292
  71.9 74.9 %copy-start.3 = (bf16[24,192]{1,0:T(8,128)(2,1)S(1)}, bf16[24,192]{1,0:T(8,128)(2,1)}, u32[]{:S(2)}) copy-start(bf16[24,192]{1,0:T(8,128)(2,1)} %param.17) | copy-start | bytes 27652
  72.0 75.7 %copy-start.4 = (bf16[24,192]{1,0:T(8,128)(2,1)S(1)}, bf16[24,192]{1,0:T(8,128)(2,1)}, u32[]{:S(2)}) copy-start(bf16[24,192]{1,0:T(8,128)(2,1)} %param.16) | copy-start | bytes 27652
Sparse Core Ops, SparseCore 0:
  12.2 146.9 all-gather.1

commit v2 on v1

--- a/solution.py
+++ b/solution.py
@@ -1,6 +1,8 @@
 import jax
 import jax.numpy as jnp
 from jax import lax
+from jax.experimental import pallas as pl
+from jax.experimental.pallas import tpu as pltpu
 from jax.sharding import Mesh
 from jax.sharding import PartitionSpec as P
 
@@ -38,6 +40,50 @@
     return jnp.sum(jnp.square(direction.astype(jnp.float32)))
 
 
+LANES = 128
+
+
+def fold_kernel(scale_ref, early_ref, dir_value_ref, dir_output_ref, value_ref, output_ref):
+    columns = value_ref.shape[1]
+    at = 2 * columns
+    left = jnp.concatenate(
+        [early_ref[:, at : at + LANES], early_ref[:, at + 2 * LANES : at + 3 * LANES]], axis=1
+    )
+    update = jnp.dot(left, dir_value_ref[...], preferred_element_type=jnp.float32)
+    update = early_ref[:, :columns].astype(jnp.float32) + update * scale_ref[0]
+    value_ref[...] = update.astype(value_ref.dtype)
+    left = early_ref[:, at + LANES : at + 3 * LANES]
+    update = jnp.dot(left, dir_output_ref[...], preferred_element_type=jnp.float32)
+    update = early_ref[:, columns:at].astype(jnp.float32) + update * scale_ref[1]
+    output_ref[...] = update.astype(output_ref.dtype).T
+
+
+def fold(scales, early, dir_value, dir_output, tile):
+    rows, columns = early.shape[0], dir_value.shape[1]
+    gap = jnp.zeros((2 * LANES - dir_value.shape[0], columns), dir_value.dtype)
+    wide_value = jnp.concatenate([dir_value, gap], axis=0)
+    wide_output = jnp.concatenate([dir_output[:LANES], gap, dir_output[LANES:]], axis=0)
+    return pl.pallas_call(
+        fold_kernel,
+        grid=(rows // tile,),
+        in_specs=[
+            pl.BlockSpec(memory_space=pltpu.SMEM),
+            pl.BlockSpec((tile, early.shape[1]), lambda i: (i, 0)),
+            pl.BlockSpec((2 * LANES, columns), lambda i: (0, 0)),
+            pl.BlockSpec((2 * LANES, columns), lambda i: (0, 0)),
+        ],
+        out_specs=[
+            pl.BlockSpec((tile, columns), lambda i: (i, 0)),
+            pl.BlockSpec((columns, tile), lambda i: (0, i)),
+        ],
+        out_shape=[
+            jax.ShapeDtypeStruct((rows, columns), jnp.bfloat16),
+            jax.ShapeDtypeStruct((columns, rows), jnp.bfloat16),
+        ],
+        name="fold",
+    )(scales, early, wide_value, wide_output)
+
+
 def per_device(
     inputs,
     value_cot,
@@ -55,32 +101,38 @@
     bf16 = jnp.bfloat16
     rank = proj_value.shape[1]
     columns = value_cot.shape[1]
-    early = jnp.concatenate(
-        [w_value.astype(bf16), w_output.T.astype(bf16), proj_value, proj_output], axis=1
-    )
-    early = lax.all_gather(early, FS, axis=0, tiled=True)
-    wide_value = early[:, :columns]
-    wide_output = early[:, columns : 2 * columns]
-    full_value = early[:, 2 * columns : 2 * columns + rank]
-    full_output = early[:, 2 * columns + rank :]
-
     width = rank // lax.axis_size("tp")
     offset = lax.axis_index("tp") * width
-    own = jnp.concatenate(
+
+    near = spread(jnp.concatenate([proj_value, proj_output], axis=1), "fs_1")
+    near = near.reshape(-1, 2 * rank)
+    old = spread(jnp.concatenate([w_value.astype(bf16), w_output.T.astype(bf16)], axis=1), "fs_1")
+    old = old.reshape(-1, 2 * columns)
+    early = jnp.concatenate(
         [
-            lax.dynamic_slice_in_dim(proj_value, offset, width, 1),
-            lax.dynamic_slice_in_dim(proj_output, offset, width, 1),
+            old,
+            near[:, :LANES],
+            near[:, rank : rank + LANES],
+            near[:, LANES:rank],
+            near[:, rank + LANES :],
         ],
         axis=1,
     )
-    rows = spread(own, "fs_0")
-    rows = spread(rows.reshape(-1, 2 * width), "fs_1")
-    rows = rows.reshape(lax.axis_size("fs_1"), lax.axis_size("fs_0"), -1, 2 * width)
-    rows = jnp.swapaxes(rows, 0, 1).reshape(-1, 2 * width)
+    early = lax.all_gather(early, "fs_0", axis=0, tiled=True)
+
+    own = jnp.concatenate(
+        [
+            lax.dynamic_slice_in_dim(near[:, :rank], offset, width, 1),
+            lax.dynamic_slice_in_dim(near[:, rank:], offset, width, 1),
+        ],
+        axis=1,
+    )
+    rows = spread(own.T, "fs_0")
+    rows = jnp.swapaxes(rows, 0, 1).reshape(2 * width, -1)
     narrow = jnp.concatenate(
         [
-            contract(rows[:, :width], inputs, ((0,), (1,))),
-            contract(rows[:, width:], output_cot, ((0,), (1,))),
+            contract(rows[:width], inputs, ((1,), (1,))),
+            contract(rows[width:], output_cot, ((1,), (1,))),
         ],
         axis=0,
     ).astype(bf16)
@@ -101,15 +153,11 @@
     dir_value, dir_output = (dirs[:, :columns], dirs[:, columns:])
     sums = jnp.stack([squares(dir_value), squares(dir_output)])
     totals = spread(sums[None], "tp").sum(axis=(0, 1))
-    scale_value = lax.rsqrt(totals[0] / (RANK * HV) + norm_eps)
-    scale_output = lax.rsqrt(totals[1] / (RANK * HV) + norm_eps)
+    scales = lax.rsqrt(totals / (RANK * HV) + norm_eps)
 
-    step_value = contract(proj_value, dir_value, ((1,), (0,))) * scale_value
-    step_output = contract(dir_output, proj_output, ((0,), (1,))) * scale_output
-    copy_value = contract(full_value, dir_value, ((1,), (0,))) * scale_value
-    copy_value = (wide_value.astype(jnp.float32) + copy_value).astype(bf16)
-    copy_output = contract(dir_output, full_output, ((0,), (1,))) * scale_output
-    copy_output = (wide_output.T.astype(jnp.float32) + copy_output).astype(bf16)
+    step_value = contract(proj_value, dir_value, ((1,), (0,))) * scales[0]
+    step_output = contract(dir_output, proj_output, ((0,), (1,))) * scales[1]
+    copy_value, copy_output = fold(scales, early, dir_value, dir_output, 768)
     return (step_value, step_output, copy_value, copy_output, first_v, second_v, first_o, second_o)
 
 

time: 180 us -> 192 us (1.067); the launches traced: 179 us -> 188 us
  blocking collectives: 124 us -> 75.4 us
  waiting for transfers between devices: 10.8 us -> 49 us
  starting transfers between devices: 0.04 us -> 22.8 us
  matrix products: 13.6 us -> 5.84 us
  Pallas kernels: 0 us -> 6.39 us
    all_to_all x6 -> x3, blocking collectives: 124 us -> 75.4 us  [exchange(): return lax.all_to_all(pieces, axis, split_axis=0, concat_axis=0, tiled=True)]
    all_to_all x0 -> x4, waiting for transfers between devices: none -> 49 us  [exchange(): return lax.all_to_all(pieces, axis, split_axis=0, concat_axis=0, tiled=True)]
    all_to_all x0 -> x4, starting transfers between devices: none -> 22.7 us  [exchange(): return lax.all_to_all(pieces, axis, split_axis=0, concat_axis=0, tiled=True)]
    all_gather x1, waiting for transfers between devices: 10.8 us -> 0.01 us  [per_device(): early = lax.all_gather(early, 'fs_0', axis=0, tiled=True)]
    dot_general x8 -> x6, matrix products: 13.6 us -> 5.84 us  [contract(): lax.dot_general(left, right, (dims, ((), ())), preferred_element_type=jnp...]
    pallas_call x0 -> x1, Pallas kernels: none -> 6.39 us  [fold(): pl.pallas_call(fold_kernel, grid=(rows // tile,), in_specs=[pl.BlockSpec(...]
    unnamed x21 -> x20, local copies, waits for them, and re-layouts: 5.06 us -> 1.03 us
    broadcast_in_dim x5 -> x6, local copies, waits for them, and re-layouts: 0.29 us -> 3.06 us  [spread(): jnp.broadcast_to(value, (lax.axis_size(axis), *value.shape))]
  transfers between devices with their start and end apart: 1 -> 5, of which waited for: 1 -> 4; matrix products, arithmetic and copies ran while one was open for 6% -> 9% of each run, Pallas kernels for 0% -> 0%
where the time goes in v2:
time: 192 us; the launch traced here: 188 us
  blocking collectives  75.4 us (39%)
  waiting for transfers between devices  49 us (26%)
  starting transfers between devices  22.8 us (12%)
  between operations  14.3 us (7%)
  local copies, waits for them, and re-layouts  8.03 us (4%)
  other arithmetic  6.64 us (3%)
  Pallas kernels  6.39 us (3%)
  matrix products  5.84 us (3%)
    all_to_all x3, blocking collectives, exchange(): return lax.all_to_all(pieces, axis, split_axis=0, concat_axis=0, tiled=True)  75.4 us
    all_to_all x4, waiting for transfers between devices, exchange(): return lax.all_to_all(pieces, axis, split_axis=0, concat_axis=0, tiled=True)  49 us
    all_to_all x4, starting transfers between devices, exchange(): return lax.all_to_all(pieces, axis, split_axis=0, concat_axis=0, tiled=True)  22.7 us
    pallas_call x1, Pallas kernels, fold(): pl.pallas_call(fold_kernel, grid=(rows // tile,), in_specs=[pl.BlockSpec(...  6.39 us
    dot_general x6, matrix products, contract(): lax.dot_general(left, right, (dims, ((), ())), preferred_element_type=jnp...  5.84 us
  transfers between devices with their start and end apart: 5, of which 4 were waited for; matrix products, arithmetic and copies ran while one was open for 9% of the time, Pallas kernels for 0%

profile of v2, /device:TPU:6, one launch (start us, length us, event | category | flops | bytes accessed | tf_op | source)
XLA Modules:
  0.0 188.4 jit_solution(1398687555496970342)
XLA Ops:
  7.2 1.0 pad_maximum_fusion.4
  8.1 0.7 broadcast_in_dim.22
  8.8 7.1 %all-to-all-start = ((bf16[8,24,384]{2,1,0:T(8,128)(2,1)}), bf16[8,24,384]{2,1,0:T(8,128)(2,1)S(1)}, u32[]{:S(2)}, u32[]{:S(2)}) async-start(bf16[8,24,384]{2,1,0:T(8,128)(2,1)} %broadcast_in_dim.22), calls=%async_computation | async-start | bytes 294912 | tf_op jit(solution)/shard_map/all_to_all | solution.py:21
  15.9 0.8 convert_element_type.32
  16.7 0.8 convert_bitcast_fusion
  17.5 7.8 %all-to-all-done = bf16[8,24,384]{2,1,0:T(8,128)(2,1)S(1)} async-done(((bf16[8,24,384]{2,1,0:T(8,128)(2,1)}), bf16[8,24,384]{2,1,0:T(8,128)(2,1)S(1)}, u32[]{:S(2)}, u32[]{:S(2)}) %all-to-all-start) | async-done | bytes 147488 | tf_op jit(solution)/shard_map/all_to_all | solution.py:21
  25.3 0.8 broadcast_in_dim.27
  26.1 3.5 %all-to-all-start.6 = ((bf16[8,24,1024]{2,1,0:T(8,128)(2,1)}), bf16[8,24,1024]{2,1,0:T(8,128)(2,1)S(1)}, u32[]{:S(2)}, u32[]{:S(2)}) async-start(bf16[8,24,1024]{2,1,0:T(8,128)(2,1)} %broadcast_in_dim.27), calls=%async_computation.6 | async-start | bytes 786432 | tf_op jit(solution)/shard_map/all_to_all | solution.py:21
  29.6 0.0 all-gather.2.cloned.1.call-start
  29.6 0.1 fusion.15
  29.7 0.1 fusion.16
  29.8 12.9 %all-to-all-done.6 = bf16[8,24,1024]{2,1,0:T(8,128)(2,1)S(1)} async-done(((bf16[8,24,1024]{2,1,0:T(8,128)(2,1)}), bf16[8,24,1024]{2,1,0:T(8,128)(2,1)S(1)}, u32[]{:S(2)}, u32[]{:S(2)}) %all-to-all-start.6) | async-done | bytes 393248 | tf_op jit(solution)/shard_map/all_to_all | solution.py:21
  42.7 0.9 concatenate.36
  43.6 0.0 all-gather.2.cloned.1.call-update
  43.6 0.1 fusion.17
  43.7 0.1 constant_dynamic-slice_fusion
  43.9 0.1 maximum_bitcast_fusion
  44.0 0.1 copy.36
  44.1 31.4 %all_to_all.35 = bf16[12,48,192]{2,1,0:T(8,128)(2,1)S(1)} all-to-all(bf16[12,48,192]{2,1,0:T(8,128)(2,1)S(1)} %broadcast_in_dim.23), channel_id=1, replica_groups=mesh['fs_0'=12,'fs_1'=8,'tp'=8] {'fs_0'}, dimensions={0} | all-to-all | bytes 442368 | tf_op jit(solution)/shard_map/all_to_all | solution.py:21
  75.6 0.2 slice.65
  75.8 0.2 slice.67
  76.0 0.7 convolution_convert_fusion.3
  76.7 1.0 copy-done.1
  77.7 0.7 convolution_convert_fusion.2
  78.5 11.4 %all_to_all.36 = bf16[8,48,512]{2,1,0:T(8,128)(2,1)S(1)} all-to-all(bf16[8,48,512]{2,1,0:T(8,128)(2,1)S(1)} %broadcast_in_dim.24), channel_id=1, replica_groups=mesh['fs_0'=12,'fs_1'=8,'tp'=8] {'tp'}, dimensions={0} | all-to-all | bytes 786432 | tf_op jit(solution)/shard_map/all_to_all | solution.py:21
  89.9 0.1 dot_general.24
  90.0 0.1 dot_general.26
  90.1 0.3 convolution_convert_fusion.1
  90.4 1.3 convolution_convert_fusion
  91.8 0.4 copy.41
  92.2 32.6 %all_to_all.37 = bf16[96,2,1024]{2,1,0:T(2,128)(2,1)S(1)} all-to-all(bf16[96,2,1024]{2,1,0:T(2,128)(2,1)S(1)} %copy.41), channel_id=1, replica_groups=mesh['fs_0'=12,'fs_1'=8,'tp'=8] {'fs_0','fs_1'}, dimensions={0} | all-to-all | bytes 786432 | tf_op jit(solution)/shard_map/all_to_all | solution.py:21
  124.8 0.4 convert_reduce_fusion
  125.1 0.6 fusion.8
  125.8 1.0 broadcast_in_dim.25
  126.7 6.8 %all-to-all-start.4 = ((bf16[96,2,1024]{2,1,0:T(2,128)(2,1)}), bf16[96,2,1024]{2,1,0:T(2,128)(2,1)S(1)}, u32[]{:S(2)}, u32[]{:S(2)}) async-start(bf16[96,2,1024]{2,1,0:T(2,128)(2,1)} %broadcast_in_dim.25), calls=%async_computation.4 | async-start | bytes 786432 | tf_op jit(solution)/shard_map/all_to_all | solution.py:21
  133.6 26.7 %all-to-all-done.4 = bf16[96,2,1024]{2,1,0:T(2,128)(2,1)S(1)} async-done(((bf16[96,2,1024]{2,1,0:T(2,128)(2,1)}), bf16[96,2,1024]{2,1,0:T(2,128)(2,1)S(1)}, u32[]{:S(2)}, u32[]{:S(2)}) %all-to-all-start.4) | async-done | bytes 393248 | tf_op jit(solution)/shard_map/all_to_all | solution.py:21
  160.3 0.1 reshape.38
  160.5 0.7 multiply_reduce_fusion.1
  161.3 1.4 pad_maximum_fusion.6
  162.6 0.6 broadcast_in_dim.26
  163.2 5.4 %all-to-all-start.5 = ((f32[8,1,2]{2,1,0:T(1,128)}), f32[8,1,2]{2,1,0:T(1,128)S(1)}, u32[]{:S(2)}, u32[]{:S(2)}) async-start(f32[8,1,2]{2,1,0:T(1,128)} %broadcast_in_dim.26), calls=%async_computation.5 | async-start | bytes 8192 | tf_op jit(solution)/shard_map/all_to_all | solution.py:21
  168.6 0.8 pad_maximum_fusion.1.dir_output_ref
  169.4 0.7 concatenate.37.dir_value_ref
  170.1 1.6 all-to-all-done.5
  171.7 0.6 fusion.18
  172.3 1.4 convolution_multiply_fusion
  173.7 1.4 fusion
  175.2 6.4 %fold.1 = (bf16[2304,512]{1,0:T(8,128)(2,1)}, bf16[512,2304]{1,0:T(8,128)(2,1)}) custom-call(f32[2]{0:T(128)} %copy-done.5, bf16[2304,1408]{1,0:T(8,128)(2,1)} %all-gather.2.cloned.1.call-done.early_ref, bf16[256,512]{1,0:T(8,128)(2,1)} %concatenate.37.dir_value_ref, bf16[256,512]{1,0:T(8,128)(2,1)} %pad_maximum_fusion.1.dir_output_ref), custom_call_target="tpu_custom_call" | custom-call | tf_op jit(solution)/shard_map/fold/pallas_call | solution.py:66
  (37 shorter events, 0.4 us)
Async XLA Ops:
  7.2 68.8 %copy-start = (bf16[512,2304]{1,0:T(8,128)(2,1)S(1)}, bf16[512,2304]{1,0:T(8,128)(2,1)}, u32[]{:S(2)}) copy-start(bf16[512,2304]{1,0:T(8,128)(2,1)} %param.12) | copy-start | bytes 7077892
  8.8 16.5 %all-to-all-start = ((bf16[8,24,384]{2,1,0:T(8,128)(2,1)}), bf16[8,24,384]{2,1,0:T(8,128)(2,1)S(1)}, u32[]{:S(2)}, u32[]{:S(2)}) async-start(bf16[8,24,384]{2,1,0:T(8,128)(2,1)} %broadcast_in_dim.22), calls=%async_computation | async-start | bytes 294912 | tf_op jit(solution)/shard_map/all_to_all | solution.py:21
  26.1 16.5 %all-to-all-start.6 = ((bf16[8,24,1024]{2,1,0:T(8,128)(2,1)}), bf16[8,24,1024]{2,1,0:T(8,128)(2,1)S(1)}, u32[]{:S(2)}, u32[]{:S(2)}) async-start(bf16[8,24,1024]{2,1,0:T(8,128)(2,1)} %broadcast_in_dim.27), calls=%async_computation.6 | async-start | bytes 786432 | tf_op jit(solution)/shard_map/all_to_all | solution.py:21
  29.6 145.6 %all-gather.2.cloned.1.call-start = ((), (), s32[]{:S(2)}) async-start(), calls=%async_computation.7 | async-start | bytes 7028736 | tf_op jit(solution)/shard_map/all_gather | solution.py:121
  76.0 1.7 copy-start.1
  77.7 12.4 %copy-start.2 = (bf16[512,512]{1,0:T(8,128)(2,1)S(1)}, bf16[512,512]{1,0:T(8,128)(2,1)}, u32[]{:S(2)}) copy-start(bf16[512,512]{1,0:T(8,128)(2,1)} %param.13) | copy-start | bytes 1572868
  90.1 35.0 %copy-start.6 = (f32[2,512]{1,0:T(2,128)S(1)}, f32[2,512]{1,0:T(2,128)}, u32[]{:S(2)}) copy-start(f32[2,512]{1,0:T(2,128)} %param.21) | copy-start | bytes 12292
  90.1 35.0 %copy-start.7 = (f32[2,512]{1,0:T(2,128)S(1)}, f32[2,512]{1,0:T(2,128)}, u32[]{:S(2)}) copy-start(f32[2,512]{1,0:T(2,128)} %param.20) | copy-start | bytes 12292
  90.1 35.0 %copy-start.8 = (f32[2,512]{1,0:T(2,128)S(1)}, f32[2,512]{1,0:T(2,128)}, u32[]{:S(2)}) copy-start(f32[2,512]{1,0:T(2,128)} %param.23) | copy-start | bytes 12292
  90.1 35.0 %copy-start.9 = (f32[2,512]{1,0:T(2,128)S(1)}, f32[2,512]{1,0:T(2,128)}, u32[]{:S(2)}) copy-start(f32[2,512]{1,0:T(2,128)} %param.22) | copy-start | bytes 12292
  124.7 47.6 %copy-start.3 = (bf16[24,192]{1,0:T(8,128)(2,1)S(1)}, bf16[24,192]{1,0:T(8,128)(2,1)}, u32[]{:S(2)}) copy-start(bf16[24,192]{1,0:T(8,128)(2,1)} %param.17) | copy-start | bytes 27652
  124.8 49.0 %copy-start.4 = (bf16[24,192]{1,0:T(8,128)(2,1)S(1)}, bf16[24,192]{1,0:T(8,128)(2,1)}, u32[]{:S(2)}) copy-start(bf16[24,192]{1,0:T(8,128)(2,1)} %param.16) | copy-start | bytes 27652
  126.7 33.6 %all-to-all-start.4 = ((bf16[96,2,1024]{2,1,0:T(2,128)(2,1)}), bf16[96,2,1024]{2,1,0:T(2,128)(2,1)S(1)}, u32[]{:S(2)}, u32[]{:S(2)}) async-start(bf16[96,2,1024]{2,1,0:T(2,128)(2,1)} %broadcast_in_dim.25), calls=%async_computation.4 | async-start | bytes 786432 | tf_op jit(solution)/shard_map/all_to_all | solution.py:21
  163.2 8.5 %all-to-all-start.5 = ((f32[8,1,2]{2,1,0:T(1,128)}), f32[8,1,2]{2,1,0:T(1,128)S(1)}, u32[]{:S(2)}, u32[]{:S(2)}) async-start(f32[8,1,2]{2,1,0:T(1,128)} %broadcast_in_dim.26), calls=%async_computation.5 | async-start | bytes 8192 | tf_op jit(solution)/shard_map/all_to_all | solution.py:21
  171.7 3.4 %copy-start.5 = (f32[2]{0:T(128)}, f32[2]{0:T(128)S(1)}, u32[]{:S(2)}) copy-start(f32[2]{0:T(128)S(1)} %add_rsqrt_fusion.scale_ref) | copy-start | bytes 28
Sparse Core Ops, SparseCore 0:
  43.8 115.7 all-gather.1

commit v3 on v2

v3 whole, which is shorter than its diff:
```python
import functools

import jax
import jax.numpy as jnp
from jax import lax
from jax.experimental import pallas as pl
from jax.experimental.pallas import tpu as pltpu
from jax.sharding import Mesh
from jax.sharding import PartitionSpec as P

RANK = 192
HV = 4096
FS = ("fs_0", "fs_1")


beta_one = 0.8
beta_two = 0.9
moment_eps = 1e-08
norm_eps = 1e-06


def exchange(pieces, axis):
    return lax.all_to_all(pieces, axis, split_axis=0, concat_axis=0, tiled=True)


def spread(value, axis):
    return exchange(jnp.broadcast_to(value, (lax.axis_size(axis), *value.shape)), axis)


def contract(left, right, dims):
    return lax.dot_general(left, right, (dims, ((), ())), preferred_element_type=jnp.float32)


def adapt(first, second, grad):
    new_first = beta_one * first + (1.0 - beta_one) * grad
    new_second = beta_two * second + (1.0 - beta_two) * grad * grad
    direction = (new_first / (jnp.sqrt(new_second) + moment_eps)).astype(jnp.bfloat16)
    return (new_first, new_second, direction)


LANES = 128


def fold_kernel(
    count,
    sums_ref,
    early_ref,
    own_value_ref,
    own_output_ref,
    wide_value_ref,
    wide_output_ref,
    dirs_ref,
    value_ref,
    output_ref,
    step_value_ref,
    step_output_ref,
):
    columns = value_ref.shape[1]
    at = 2 * columns

    def scale_of(sums):
        total = jnp.sum(jnp.sum(sums, axis=1, keepdims=True), axis=0, keepdims=True)
        return lax.rsqrt(total / count + norm_eps)

    scale_value = scale_of(sums_ref[:, :columns])
    scale_output = scale_of(sums_ref[:, columns:])

    @pl.when(pl.program_id(0) == 0)
    def _():
        step = jnp.dot(
            own_value_ref[...], dirs_ref[:, :columns], preferred_element_type=jnp.float32
        )
        step_value_ref[...] = step * scale_value
        step = jnp.dot(
            own_output_ref[...], dirs_ref[:, columns:], preferred_element_type=jnp.float32
        )
        step_output_ref[...] = step * scale_output

    left = jnp.concatenate(
        [early_ref[:, at : at + LANES], early_ref[:, at + 2 * LANES : at + 3 * LANES]], axis=1
    )
    update = jnp.dot(left, wide_value_ref[...], preferred_element_type=jnp.float32)
    update = early_ref[:, :columns].astype(jnp.float32) + update * scale_value
    value_ref[...] = update.astype(value_ref.dtype)
    left = early_ref[:, at + LANES : at + 3 * LANES]
    update = jnp.dot(left, wide_output_ref[...], preferred_element_type=jnp.float32)
    update = early_ref[:, columns:at].astype(jnp.float32) + update * scale_output
    output_ref[...] = update.astype(output_ref.dtype).T


def fold(sums, early, proj_value, proj_output, dirs, tile):
    rows, columns = early.shape[0], dirs.shape[1] // 2
    own, rank = proj_value.shape
    gap = jnp.zeros((2 * LANES - rank, columns), dirs.dtype)
    wide_value = jnp.concatenate([dirs[:, :columns], gap], axis=0)
    wide_output = jnp.concatenate([dirs[:LANES, columns:], gap, dirs[LANES:, columns:]], axis=0)

    def whole(*shape):
        return pl.BlockSpec(shape, lambda i: (0, 0))

    out = pl.pallas_call(
        functools.partial(fold_kernel, RANK * HV),
        grid=(rows // tile,),
        in_specs=[
            whole(*sums.shape),
            pl.BlockSpec((tile, early.shape[1]), lambda i: (i, 0)),
            whole(own, rank),
            whole(own, rank),
            whole(2 * LANES, columns),
            whole(2 * LANES, columns),
            whole(rank, 2 * columns),
        ],
        out_specs=[
            pl.BlockSpec((tile, columns), lambda i: (i, 0)),
            pl.BlockSpec((columns, tile), lambda i: (0, i)),
            whole(own, columns),
            whole(own, columns),
        ],
        out_shape=[
            jax.ShapeDtypeStruct((rows, columns), jnp.bfloat16),
            jax.ShapeDtypeStruct((columns, rows), jnp.bfloat16),
            jax.ShapeDtypeStruct((own, columns), jnp.float32),
            jax.ShapeDtypeStruct((own, columns), jnp.float32),
        ],
        name="fold",
    )(sums, early, proj_value, proj_output, wide_value, wide_output, dirs)
    return (out[0], out[1], out[2], out[3].T)


def per_device(
    inputs,
    value_cot,
    retained,
    output_cot,
    proj_value,
    proj_output,
    w_value,
    w_output,
    first_value,
    second_value,
    first_output,
    second_output,
):
    bf16 = jnp.bfloat16
    rank = proj_value.shape[1]
    columns = value_cot.shape[1]
    deep, high = lax.axis_size("fs_0"), lax.axis_size("fs_1")

    piece = [w_value.astype(bf16), w_output.T.astype(bf16)]
    piece += [proj_value[:, :LANES], proj_output[:, :LANES]]
    piece += [proj_value[:, LANES:], proj_output[:, LANES:]]
    near = spread(jnp.concatenate(piece, axis=1), "fs_1")
    near = near.reshape(-1, near.shape[-1])
    early = lax.all_gather(near, "fs_0", axis=0, tiled=True)

    width = rank // lax.axis_size("tp")
    offset = lax.axis_index("tp") * width
    at, rest = 2 * columns, rank - LANES
    last = at + 2 * LANES
    near_value = jnp.concatenate([near[:, at : at + LANES], near[:, last : last + rest]], axis=1)
    near_output = jnp.concatenate([near[:, at + LANES : last], near[:, last + rest :]], axis=1)
    own = jnp.concatenate(
        [
            lax.dynamic_slice_in_dim(near_value, offset, width, 1),
            lax.dynamic_slice_in_dim(near_output, offset, width, 1),
        ],
        axis=1,
    )
    rows = spread(own.T, "fs_0")
    rows = jnp.swapaxes(rows, 0, 1).reshape(2 * width, -1)
    narrow = jnp.concatenate(
        [
            contract(rows[:width], inputs, ((1,), (1,))),
            contract(rows[width:], output_cot, ((1,), (1,))),
        ],
        axis=0,
    ).astype(bf16)
    projected = spread(narrow, "tp")
    x_proj = projected[:, :width].reshape(rank, -1)
    o_proj = projected[:, width:].reshape(rank, -1)

    partial = jnp.concatenate(
        [contract(x_proj, value_cot, ((1,), (0,))), contract(o_proj, retained, ((1,), (0,)))],
        axis=1,
    ).astype(bf16)
    pieces = partial.reshape(deep, high, -1, 2 * columns)
    pieces = exchange(jnp.swapaxes(pieces, 0, 1).reshape(high, -1, 2 * columns), "fs_1")
    pieces = pieces.astype(jnp.float32).sum(axis=0).astype(bf16)
    pieces = exchange(pieces.reshape(deep, -1, 2 * columns), "fs_0")
    summed = pieces.astype(jnp.float32).sum(axis=0)
    first_v, second_v, dir_value = adapt(first_value, second_value, summed[:, :columns])
    first_o, second_o, dir_output = adapt(first_output, second_output, summed[:, columns:])

    dirs = spread(jnp.concatenate([dir_value, dir_output], axis=1), "fs_0")
    dirs = spread(dirs.reshape(-1, 2 * columns), "fs_1")
    sums = jnp.square(dirs.astype(jnp.float32)).sum(axis=(0, 1))
    sums = spread(sums, "tp")
    dirs = dirs.reshape(high, deep, -1, 2 * columns)
    dirs = jnp.swapaxes(dirs, 0, 1).reshape(rank, -1)

    copy_value, copy_output, step_value, step_output = fold(
        sums, early, proj_value, proj_output, dirs, 768
    )
    return (step_value, step_output, copy_value, copy_output, first_v, second_v, first_o, second_o)


def solution(mesh):
    split = Mesh(mesh.devices.reshape(12, 8, mesh.shape["tp"]), ("fs_0", "fs_1", "tp"))
    return jax.shard_map(
        per_device,
        mesh=split,
        in_specs=(
            P(FS, None),
            P(FS, "tp"),
            P(FS, "tp"),
            P(FS, None),
            P(FS, None),
            P(FS, None),
            P(FS, "tp"),
            P("tp", FS),
            P(FS, "tp"),
            P(FS, "tp"),
            P(FS, "tp"),
            P(FS, "tp"),
        ),
        out_specs=(
            P(FS, "tp"),
            P("tp", FS),
            P(None, "tp"),
            P("tp", None),
            P(FS, "tp"),
            P(FS, "tp"),
            P(FS, "tp"),
            P(FS, "tp"),
        ),
        check_vma=False,
    )
```

time: 192 us -> 179 us (0.932)
  blocking collectives: 75.4 us -> 116 us
  waiting for transfers between devices: 49 us -> 13.6 us
  starting transfers between devices: 22.8 us -> 8.7 us
  other arithmetic: 6.64 us -> 3.54 us
  matrix products: 5.84 us -> 3.01 us
  local copies, waits for them, and re-layouts: 8.03 us -> 10.5 us
    all_to_all x3 -> x6, blocking collectives: 75.4 us -> 116 us  [exchange(): return lax.all_to_all(pieces, axis, split_axis=0, concat_axis=0, tiled=True)]
    all_to_all x4 -> x2, waiting for transfers between devices: 49 us -> 13.6 us  [exchange(): return lax.all_to_all(pieces, axis, split_axis=0, concat_axis=0, tiled=True)]
    all_to_all x4 -> x2, starting transfers between devices: 22.7 us -> 8.66 us  [exchange(): return lax.all_to_all(pieces, axis, split_axis=0, concat_axis=0, tiled=True)]
    slice x7 -> x9, local copies, waits for them, and re-layouts: 0.89 us -> 4.74 us  [the longest x2 1.54 us: per_device(): piece += [proj_value[:, :LANES], proj_output[:, :LANES]]]
    dot_general x6 -> x4, matrix products: 5.84 us -> 3.01 us  [contract(): lax.dot_general(left, right, (dims, ((), ())), preferred_element_type=jnp...]
  transfers between devices with their start and end apart: 5 -> 3, of which waited for: 4 -> 2; matrix products, arithmetic and copies ran while one was open for 9% -> 6% of each run, Pallas kernels for 0% -> 0%
where the time goes in v3:
time: 179 us; the launch traced here: 176 us
  blocking collectives  116 us (65%)
  between operations  14.4 us (8%)
  waiting for transfers between devices  13.6 us (8%)
  local copies, waits for them, and re-layouts  10.5 us (6%)
  starting transfers between devices  8.7 us (5%)
  Pallas kernels  6.91 us (4%)
  other arithmetic  3.54 us (2%)
  matrix products  3.01 us (2%)
    all_to_all x6, blocking collectives, exchange(): return lax.all_to_all(pieces, axis, split_axis=0, concat_axis=0, tiled=True)  116 us
    all_to_all x2, waiting for transfers between devices, exchange(): return lax.all_to_all(pieces, axis, split_axis=0, concat_axis=0, tiled=True)  13.6 us
    all_to_all x2, starting transfers between devices, exchange(): return lax.all_to_all(pieces, axis, split_axis=0, concat_axis=0, tiled=True)  8.66 us
    pallas_call x1, Pallas kernels, fold(): pl.pallas_call(functools.partial(fold_kernel, RANK * HV), grid=(rows // t...  6.91 us
  transfers between devices with their start and end apart: 3, of which 2 were waited for; matrix products, arithmetic and copies ran while one was open for 6% of the time, Pallas kernels for 0%

profile of v3, /device:TPU:6, one launch (start us, length us, event | category | flops | bytes accessed | tf_op | source)
XLA Modules:
  0.0 176.2 jit_solution(9922416823727033793)
XLA Ops:
  7.2 0.0 copy-start
  7.2 0.0 all-gather.2.cloned.1.call-start
  7.2 0.8 slice.57
  8.1 0.7 slice.59
  8.8 0.7 slice.58
  9.5 0.7 slice.60
  10.2 0.8 convert_element_type.26
  11.0 0.8 convert_bitcast_fusion
  11.8 0.1 concatenate.30
  11.9 24.8 %all_to_all.43 = bf16[8,24,1408]{2,1,0:T(8,128)(2,1)} all-to-all(bf16[8,24,1408]{2,1,0:T(8,128)(2,1)S(1)} %broadcast_in_dim.21), channel_id=1, replica_groups=mesh['fs_0'=12,'fs_1'=8,'tp'=8] {'fs_1'}, dimensions={0} | all-to-all | bytes 1081344 | tf_op jit(solution)/shard_map/all_to_all | solution.py:23
  36.7 0.0 all-gather.2.cloned.1.call-update
  36.8 1.0 fusion.12
  37.7 0.8 fusion.13
  38.6 0.1 fusion.4
  38.7 0.1 maximum_bitcast_fusion
  38.8 0.1 copy.33
  38.9 34.2 %all_to_all.44 = bf16[12,48,192]{2,1,0:T(8,128)(2,1)S(1)} all-to-all(bf16[12,48,192]{2,1,0:T(8,128)(2,1)S(1)} %broadcast_in_dim.22), channel_id=1, replica_groups=mesh['fs_0'=12,'fs_1'=8,'tp'=8] {'fs_0'}, dimensions={0} | all-to-all | bytes 442368 | tf_op jit(solution)/shard_map/all_to_all | solution.py:23
  73.2 0.2 slice.66
  73.4 0.2 slice.68
  73.6 0.7 convolution_convert_fusion.3
  74.3 0.9 copy-done.2
  75.3 0.7 convolution_convert_fusion.2
  76.0 11.4 %all_to_all.45 = bf16[8,48,512]{2,1,0:T(8,128)(2,1)S(1)} all-to-all(bf16[8,48,512]{2,1,0:T(8,128)(2,1)S(1)} %broadcast_in_dim.23), channel_id=1, replica_groups=mesh['fs_0'=12,'fs_1'=8,'tp'=8] {'tp'}, dimensions={0} | all-to-all | bytes 786432 | tf_op jit(solution)/shard_map/all_to_all | solution.py:23
  87.5 0.1 dot_general.18
  87.6 0.1 dot_general.20
  87.7 0.3 convolution_convert_fusion.1
  88.0 1.3 convolution_convert_fusion
  89.3 0.2 copy.38
  89.6 17.2 %all_to_all.46 = bf16[8,24,1024]{2,1,0:T(8,128)(2,1)S(1)} all-to-all(bf16[8,24,1024]{2,1,0:T(8,128)(2,1)S(1)} %copy.38), channel_id=1, replica_groups=mesh['fs_0'=12,'fs_1'=8,'tp'=8] {'fs_1'}, dimensions={0} | all-to-all | bytes 786432 | tf_op jit(solution)/shard_map/all_to_all | solution.py:23
  106.8 0.1 reduce_sum.30
  106.9 14.0 %all_to_all.47 = bf16[12,2,1024]{2,1,0:T(2,128)(2,1)S(1)} all-to-all(bf16[12,2,1024]{2,1,0:T(2,128)(2,1)S(1)} %reshape.52), channel_id=1, replica_groups=mesh['fs_0'=12,'fs_1'=8,'tp'=8] {'fs_0'}, dimensions={0} | all-to-all | bytes 98304 | tf_op jit(solution)/shard_map/all_to_all | solution.py:23
  120.9 0.1 convert_reduce_fusion
  121.0 0.6 fusion.8
  121.6 14.0 %all_to_all.48 = bf16[12,2,1024]{2,1,0:T(2,128)(2,1)S(1)} all-to-all(bf16[12,2,1024]{2,1,0:T(2,128)(2,1)S(1)} %broadcast_in_dim.24), channel_id=1, replica_groups=mesh['fs_0'=12,'fs_1'=8,'tp'=8] {'fs_0'}, dimensions={0} | all-to-all | bytes 98304 | tf_op jit(solution)/shard_map/all_to_all | solution.py:23
  135.6 0.8 broadcast_in_dim.25
  136.4 3.5 %all-to-all-start.6 = ((bf16[8,24,1024]{2,1,0:T(8,128)(2,1)}), bf16[8,24,1024]{2,1,0:T(8,128)(2,1)S(1)}, u32[]{:S(2)}, u32[]{:S(2)}) async-start(bf16[8,24,1024]{2,1,0:T(8,128)(2,1)} %broadcast_in_dim.25), calls=%async_computation.6 | async-start | bytes 786432 | tf_op jit(solution)/shard_map/all_to_all | solution.py:23
  139.9 11.8 %all-to-all-done.6 = bf16[8,24,1024]{2,1,0:T(8,128)(2,1)S(1)} async-done(((bf16[8,24,1024]{2,1,0:T(8,128)(2,1)}), bf16[8,24,1024]{2,1,0:T(8,128)(2,1)S(1)}, u32[]{:S(2)}, u32[]{:S(2)}) %all-to-all-start.6) | async-done | bytes 393248 | tf_op jit(solution)/shard_map/all_to_all | solution.py:23
  151.7 0.2 copy.39
  151.9 0.4 copy.40
  152.3 0.1 reshape.55.dirs_ref
  152.5 0.1 multiply_reduce_fusion
  152.6 0.6 broadcast_in_dim.26
  153.3 5.2 %all-to-all-start.7 = ((f32[8,1,1024]{2,1,0:T(1,128)}), f32[8,1,1024]{2,1,0:T(1,128)S(1)}, u32[]{:S(2)}, u32[]{:S(2)}) async-start(f32[8,1,1024]{2,1,0:T(1,128)} %broadcast_in_dim.26), calls=%async_computation.7 | async-start | bytes 65536 | tf_op jit(solution)/shard_map/all_to_all | solution.py:23
  158.5 0.8 pad_maximum_fusion.1.wide_output_ref
  159.3 0.7 concatenate.37.wide_value_ref
  160.0 1.8 %all-to-all-done.7 = f32[8,1,1024]{2,1,0:T(1,128)S(1)} async-done(((f32[8,1,1024]{2,1,0:T(1,128)}), f32[8,1,1024]{2,1,0:T(1,128)S(1)}, u32[]{:S(2)}, u32[]{:S(2)}) %all-to-all-start.7) | async-done | bytes 32800 | tf_op jit(solution)/shard_map/all_to_all | solution.py:23
  161.8 0.6 copy.49
  162.4 6.9 %fold.1 = (bf16[2304,512]{1,0:T(8,128)(2,1)}, bf16[512,2304]{1,0:T(8,128)(2,1)}, f32[24,512]{1,0:T(8,128)}, f32[24,512]{1,0:T(8,128)}) custom-call(f32[8,1024]{1,0:T(8,128)} %bitcast.36, bf16[2304,1408]{1,0:T(8,128)(2,1)} %all-gather.2.cloned.1.call-done.early_ref, bf16[24,192]{1,0:T(8,128)(2,1)} %own_value_ref.1, bf16[24,192]{1,0:T(8,128)(2,1)} %own_output_ref.1, ...), custom_call_target="tpu_custom_call" | custom-call | tf_op jit(solution)/shard_map/fold/pallas_call | solution.py:101
  (33 shorter events, 0.4 us)
Async XLA Ops:
  7.2 66.4 %copy-start = (bf16[512,2304]{1,0:T(8,128)(2,1)S(1)}, bf16[512,2304]{1,0:T(8,128)(2,1)}, u32[]{:S(2)}) copy-start(bf16[512,2304]{1,0:T(8,128)(2,1)} %param.12) | copy-start | bytes 7077892
  7.2 155.3 %all-gather.2.cloned.1.call-start = ((), (), s32[]{:S(2)}) async-start(), calls=%async_computation.8 | async-start | bytes 7028736 | tf_op jit(solution)/shard_map/all_gather | solution.py:154
  73.6 1.7 copy-start.2
  75.3 12.4 %copy-start.3 = (bf16[512,512]{1,0:T(8,128)(2,1)S(1)}, bf16[512,512]{1,0:T(8,128)(2,1)}, u32[]{:S(2)}) copy-start(bf16[512,512]{1,0:T(8,128)(2,1)} %param.13) | copy-start | bytes 1572868
  87.7 33.3 %copy-start.4 = (f32[2,512]{1,0:T(2,128)S(1)}, f32[2,512]{1,0:T(2,128)}, u32[]{:S(2)}) copy-start(f32[2,512]{1,0:T(2,128)} %param.21) | copy-start | bytes 12292
  87.7 33.3 %copy-start.5 = (f32[2,512]{1,0:T(2,128)S(1)}, f32[2,512]{1,0:T(2,128)}, u32[]{:S(2)}) copy-start(f32[2,512]{1,0:T(2,128)} %param.20) | copy-start | bytes 12292
  87.7 33.3 %copy-start.6 = (f32[2,512]{1,0:T(2,128)S(1)}, f32[2,512]{1,0:T(2,128)}, u32[]{:S(2)}) copy-start(f32[2,512]{1,0:T(2,128)} %param.23) | copy-start | bytes 12292
  87.7 33.2 %copy-start.7 = (f32[2,512]{1,0:T(2,128)S(1)}, f32[2,512]{1,0:T(2,128)}, u32[]{:S(2)}) copy-start(f32[2,512]{1,0:T(2,128)} %param.22) | copy-start | bytes 12292
  136.4 15.3 %all-to-all-start.6 = ((bf16[8,24,1024]{2,1,0:T(8,128)(2,1)}), bf16[8,24,1024]{2,1,0:T(8,128)(2,1)S(1)}, u32[]{:S(2)}, u32[]{:S(2)}) async-start(bf16[8,24,1024]{2,1,0:T(8,128)(2,1)} %broadcast_in_dim.25), calls=%async_computation.6 | async-start | bytes 786432 | tf_op jit(solution)/shard_map/all_to_all | solution.py:23
  152.5 10.0 %copy-start.1 = (bf16[192,1024]{1,0:T(8,128)(2,1)}, bf16[192,1024]{1,0:T(8,128)(2,1)S(1)}, u32[]{:S(2)}) copy-start(bf16[192,1024]{1,0:T(8,128)(2,1)S(1)} %reshape.55.dirs_ref) | copy-start | bytes 1179652
  153.3 8.6 %all-to-all-start.7 = ((f32[8,1,1024]{2,1,0:T(1,128)}), f32[8,1,1024]{2,1,0:T(1,128)S(1)}, u32[]{:S(2)}, u32[]{:S(2)}) async-start(f32[8,1,1024]{2,1,0:T(1,128)} %broadcast_in_dim.26), calls=%async_computation.7 | async-start | bytes 65536 | tf_op jit(solution)/shard_map/all_to_all | solution.py:23
Sparse Core Ops, SparseCore 0:
  36.9 95.8 all-gather.1

commit v4 on v3

--- a/solution.py
+++ b/solution.py
@@ -38,24 +38,19 @@
     return (new_first, new_second, direction)
 
 
-LANES = 128
-
-
 def fold_kernel(
     count,
     sums_ref,
     early_ref,
     own_value_ref,
     own_output_ref,
-    wide_value_ref,
-    wide_output_ref,
     dirs_ref,
     value_ref,
     output_ref,
     step_value_ref,
     step_output_ref,
 ):
-    columns = value_ref.shape[1]
+    columns, rank = value_ref.shape[1], own_value_ref.shape[1]
     at = 2 * columns
 
     def scale_of(sums):
@@ -76,14 +71,12 @@
         )
         step_output_ref[...] = step * scale_output
 
-    left = jnp.concatenate(
-        [early_ref[:, at : at + LANES], early_ref[:, at + 2 * LANES : at + 3 * LANES]], axis=1
-    )
-    update = jnp.dot(left, wide_value_ref[...], preferred_element_type=jnp.float32)
+    left = early_ref[:, at : at + rank]
+    update = jnp.dot(left, dirs_ref[:, :columns], preferred_element_type=jnp.float32)
     update = early_ref[:, :columns].astype(jnp.float32) + update * scale_value
     value_ref[...] = update.astype(value_ref.dtype)
-    left = early_ref[:, at + LANES : at + 3 * LANES]
-    update = jnp.dot(left, wide_output_ref[...], preferred_element_type=jnp.float32)
+    left = early_ref[:, at + rank :]
+    update = jnp.dot(left, dirs_ref[:, columns:], preferred_element_type=jnp.float32)
     update = early_ref[:, columns:at].astype(jnp.float32) + update * scale_output
     output_ref[...] = update.astype(output_ref.dtype).T
 
@@ -91,9 +84,6 @@
 def fold(sums, early, proj_value, proj_output, dirs, tile):
     rows, columns = early.shape[0], dirs.shape[1] // 2
     own, rank = proj_value.shape
-    gap = jnp.zeros((2 * LANES - rank, columns), dirs.dtype)
-    wide_value = jnp.concatenate([dirs[:, :columns], gap], axis=0)
-    wide_output = jnp.concatenate([dirs[:LANES, columns:], gap, dirs[LANES:, columns:]], axis=0)
 
     def whole(*shape):
         return pl.BlockSpec(shape, lambda i: (0, 0))
@@ -106,8 +96,6 @@
             pl.BlockSpec((tile, early.shape[1]), lambda i: (i, 0)),
             whole(own, rank),
             whole(own, rank),
-            whole(2 * LANES, columns),
-            whole(2 * LANES, columns),
             whole(rank, 2 * columns),
         ],
         out_specs=[
@@ -123,7 +111,7 @@
             jax.ShapeDtypeStruct((own, columns), jnp.float32),
         ],
         name="fold",
-    )(sums, early, proj_value, proj_output, wide_value, wide_output, dirs)
+    )(sums, early, proj_value, proj_output, dirs)
     return (out[0], out[1], out[2], out[3].T)
 
 
@@ -146,27 +134,22 @@
     columns = value_cot.shape[1]
     deep, high = lax.axis_size("fs_0"), lax.axis_size("fs_1")
 
-    piece = [w_value.astype(bf16), w_output.T.astype(bf16)]
-    piece += [proj_value[:, :LANES], proj_output[:, :LANES]]
-    piece += [proj_value[:, LANES:], proj_output[:, LANES:]]
+    piece = [w_value.astype(bf16), w_output.T.astype(bf16), proj_value, proj_output]
     near = spread(jnp.concatenate(piece, axis=1), "fs_1")
     near = near.reshape(-1, near.shape[-1])
-    early = lax.all_gather(near, "fs_0", axis=0, tiled=True)
-
     width = rank // lax.axis_size("tp")
     offset = lax.axis_index("tp") * width
-    at, rest = 2 * columns, rank - LANES
-    last = at + 2 * LANES
-    near_value = jnp.concatenate([near[:, at : at + LANES], near[:, last : last + rest]], axis=1)
-    near_output = jnp.concatenate([near[:, at + LANES : last], near[:, last + rest :]], axis=1)
+    at = 2 * columns
     own = jnp.concatenate(
         [
-            lax.dynamic_slice_in_dim(near_value, offset, width, 1),
-            lax.dynamic_slice_in_dim(near_output, offset, width, 1),
+            lax.dynamic_slice_in_dim(near[:, at : at + rank], offset, width, 1),
+            lax.dynamic_slice_in_dim(near[:, at + rank :], offset, width, 1),
         ],
         axis=1,
     )
     rows = spread(own.T, "fs_0")
+    near, rows = lax.optimization_barrier((near, rows))
+    early = lax.all_gather(near, "fs_0", axis=0, tiled=True)
     rows = jnp.swapaxes(rows, 0, 1).reshape(2 * width, -1)
     narrow = jnp.concatenate(
         [

time: 179 us -> 173 us (0.966)
  blocking collectives: 116 us -> 104 us
  waiting for transfers between devices: 13.6 us -> 19.6 us
  starting transfers between devices: 8.7 us -> 12.5 us
  local copies, waits for them, and re-layouts: 10.5 us -> 6.72 us
    all_to_all x6, blocking collectives: 116 us -> 104 us  [exchange(): return lax.all_to_all(pieces, axis, split_axis=0, concat_axis=0, tiled=True)]
    all_to_all x2, waiting for transfers between devices: 13.6 us -> 19.6 us  [exchange(): return lax.all_to_all(pieces, axis, split_axis=0, concat_axis=0, tiled=True)]
    slice x9 -> x1, local copies, waits for them, and re-layouts: 4.74 us -> 0.09 us  [per_device(): near[:, at:at + rank]]
    all_to_all x2, starting transfers between devices: 8.66 us -> 12.5 us  [exchange(): return lax.all_to_all(pieces, axis, split_axis=0, concat_axis=0, tiled=True)]
  transfers between devices with their start and end apart: 3 -> 3, of which waited for: 2 -> 2; matrix products, arithmetic and copies ran while one was open for 6% -> 5% of each run, Pallas kernels for 0% -> 0%
where the time goes in v4:
time: 173 us; the launch traced here: 170 us
  blocking collectives  104 us (60%)
  waiting for transfers between devices  19.6 us (11%)
  between operations  14.3 us (8%)
  starting transfers between devices  12.5 us (7%)
  Pallas kernels  7.12 us (4%)
  local copies, waits for them, and re-layouts  6.72 us (4%)
  matrix products  3.01 us (2%)
  other arithmetic  2.74 us (2%)
    all_to_all x6, blocking collectives, exchange(): return lax.all_to_all(pieces, axis, split_axis=0, concat_axis=0, tiled=True)  104 us
    all_to_all x2, waiting for transfers between devices, exchange(): return lax.all_to_all(pieces, axis, split_axis=0, concat_axis=0, tiled=True)  19.6 us
    all_to_all x2, starting transfers between devices, exchange(): return lax.all_to_all(pieces, axis, split_axis=0, concat_axis=0, tiled=True)  12.5 us
    pallas_call x1, Pallas kernels, fold(): pl.pallas_call(functools.partial(fold_kernel, RANK * HV), grid=(rows // t...  7.12 us
  transfers between devices with their start and end apart: 3, of which 2 were waited for; matrix products, arithmetic and copies ran while one was open for 5% of the time, Pallas kernels for 0%

profile of v4, /device:TPU:6, one launch (start us, length us, event | category | flops | bytes accessed | tf_op | source)
XLA Modules:
  0.0 169.5 jit_solution(9445593105181242307)
XLA Ops:
  7.2 0.0 copy-start
  7.2 1.0 convert_element_type.26
  8.1 0.8 convert_bitcast_fusion
  8.9 0.8 concatenate.18
  9.8 0.8 broadcast_in_dim.18
  10.6 7.1 %all-to-all-start = ((bf16[8,24,1408]{2,1,0:T(8,128)(2,1)}), bf16[8,24,1408]{2,1,0:T(8,128)(2,1)S(1)}, u32[]{:S(2)}, u32[]{:S(2)}) async-start(bf16[8,24,1408]{2,1,0:T(8,128)(2,1)} %broadcast_in_dim.18), calls=%async_computation | async-start | bytes 1081344 | tf_op jit(solution)/shard_map/all_to_all | solution.py:23
  17.7 0.0 all-gather.2.cloned.1.call-start
  17.7 17.8 %all-to-all-done = bf16[8,24,1408]{2,1,0:T(8,128)(2,1)S(1)} async-done(((bf16[8,24,1408]{2,1,0:T(8,128)(2,1)}), bf16[8,24,1408]{2,1,0:T(8,128)(2,1)S(1)}, u32[]{:S(2)}, u32[]{:S(2)}) %all-to-all-start) | async-done | bytes 540704 | tf_op jit(solution)/shard_map/all_to_all | solution.py:23
  35.5 0.1 fusion.10
  35.6 0.1 constant_dynamic-slice_fusion
  35.8 0.1 maximum_bitcast_fusion
  35.9 0.1 copy.33
  36.0 32.1 %all_to_all.43 = bf16[12,48,192]{2,1,0:T(8,128)(2,1)S(1)} all-to-all(bf16[12,48,192]{2,1,0:T(8,128)(2,1)S(1)} %broadcast_in_dim.19), channel_id=1, replica_groups=mesh['fs_0'=12,'fs_1'=8,'tp'=8] {'fs_0'}, dimensions={0} | all-to-all | bytes 442368 | tf_op jit(solution)/shard_map/all_to_all | solution.py:23
  68.1 0.0 all-gather.2.cloned.1.call-update
  68.2 0.2 slice.33
  68.4 0.2 slice.35
  68.6 0.0 copy-start.2
  68.6 0.7 convolution_convert_fusion.3
  69.3 0.9 copy-done.2
  70.3 0.7 convolution_convert_fusion.2
  71.1 11.4 %all_to_all.44 = bf16[8,48,512]{2,1,0:T(8,128)(2,1)S(1)} all-to-all(bf16[8,48,512]{2,1,0:T(8,128)(2,1)S(1)} %broadcast_in_dim.20), channel_id=1, replica_groups=mesh['fs_0'=12,'fs_1'=8,'tp'=8] {'tp'}, dimensions={0} | all-to-all | bytes 786432 | tf_op jit(solution)/shard_map/all_to_all | solution.py:23
  82.5 0.1 dot_general.18
  82.6 0.1 dot_general.20
  82.7 0.0 copy-done.3
  82.7 0.0 copy-start.4
  82.7 0.0 copy-start.5
  82.7 0.0 copy-start.6
  82.7 0.0 copy-start.7
  82.7 0.3 convolution_convert_fusion.1
  83.0 1.3 convolution_convert_fusion
  84.4 0.2 copy.38
  84.6 17.2 %all_to_all.45 = bf16[8,24,1024]{2,1,0:T(8,128)(2,1)S(1)} all-to-all(bf16[8,24,1024]{2,1,0:T(8,128)(2,1)S(1)} %copy.38), channel_id=1, replica_groups=mesh['fs_0'=12,'fs_1'=8,'tp'=8] {'fs_1'}, dimensions={0} | all-to-all | bytes 786432 | tf_op jit(solution)/shard_map/all_to_all | solution.py:23
  101.8 0.1 reduce_sum.30
  101.9 14.5 %all_to_all.46 = bf16[12,2,1024]{2,1,0:T(2,128)(2,1)S(1)} all-to-all(bf16[12,2,1024]{2,1,0:T(2,128)(2,1)S(1)} %reshape.52), channel_id=1, replica_groups=mesh['fs_0'=12,'fs_1'=8,'tp'=8] {'fs_0'}, dimensions={0} | all-to-all | bytes 98304 | tf_op jit(solution)/shard_map/all_to_all | solution.py:23
  116.4 0.1 convert_reduce_fusion
  116.5 0.0 copy-done.5
  116.5 0.6 fusion.6
  117.1 14.0 %all_to_all.47 = bf16[12,2,1024]{2,1,0:T(2,128)(2,1)S(1)} all-to-all(bf16[12,2,1024]{2,1,0:T(2,128)(2,1)S(1)} %broadcast_in_dim.21), channel_id=1, replica_groups=mesh['fs_0'=12,'fs_1'=8,'tp'=8] {'fs_0'}, dimensions={0} | all-to-all | bytes 98304 | tf_op jit(solution)/shard_map/all_to_all | solution.py:23
  131.2 14.3 %all_to_all.48 = bf16[8,24,1024]{2,1,0:T(8,128)(2,1)S(1)} all-to-all(bf16[8,24,1024]{2,1,0:T(8,128)(2,1)S(1)} %broadcast_in_dim.22), channel_id=1, replica_groups=mesh['fs_0'=12,'fs_1'=8,'tp'=8] {'fs_1'}, dimensions={0} | all-to-all | bytes 786432 | tf_op jit(solution)/shard_map/all_to_all | solution.py:23
  145.5 0.1 multiply_reduce_fusion
  145.6 0.6 broadcast_in_dim.23
  146.2 5.4 %all-to-all-start.7 = ((f32[8,1,1024]{2,1,0:T(1,128)}), f32[8,1,1024]{2,1,0:T(1,128)S(1)}, u32[]{:S(2)}, u32[]{:S(2)}) async-start(f32[8,1,1024]{2,1,0:T(1,128)} %broadcast_in_dim.23), calls=%async_computation.7 | async-start | bytes 65536 | tf_op jit(solution)/shard_map/all_to_all | solution.py:23
  151.6 0.2 copy.39
  151.8 0.4 copy.40
  152.2 0.9 reshape.55.dirs_ref
  153.1 1.8 %all-to-all-done.7 = f32[8,1,1024]{2,1,0:T(1,128)S(1)} async-done(((f32[8,1,1024]{2,1,0:T(1,128)}), f32[8,1,1024]{2,1,0:T(1,128)S(1)}, u32[]{:S(2)}, u32[]{:S(2)}) %all-to-all-start.7) | async-done | bytes 32800 | tf_op jit(solution)/shard_map/all_to_all | solution.py:23
  154.9 0.6 copy.49
  155.5 7.1 %fold.1 = (bf16[2304,512]{1,0:T(8,128)(2,1)}, bf16[512,2304]{1,0:T(8,128)(2,1)}, f32[24,512]{1,0:T(8,128)}, f32[24,512]{1,0:T(8,128)}) custom-call(f32[8,1024]{1,0:T(8,128)} %bitcast.35, bf16[2304,1408]{1,0:T(8,128)(2,1)} %all-gather.2.cloned.1.call-done.early_ref, bf16[24,192]{1,0:T(8,128)(2,1)} %own_value_ref.1, bf16[24,192]{1,0:T(8,128)(2,1)} %own_output_ref.1, ...), custom_call_target="tpu_custom_call" | custom-call | tf_op jit(solution)/shard_map/fold/pallas_call | solution.py:91
  (21 shorter events, 0.3 us)
Async XLA Ops:
  7.2 61.4 %copy-start = (bf16[512,2304]{1,0:T(8,128)(2,1)S(1)}, bf16[512,2304]{1,0:T(8,128)(2,1)}, u32[]{:S(2)}) copy-start(bf16[512,2304]{1,0:T(8,128)(2,1)} %param.12) | copy-start | bytes 7077892
  10.6 24.9 %all-to-all-start = ((bf16[8,24,1408]{2,1,0:T(8,128)(2,1)}), bf16[8,24,1408]{2,1,0:T(8,128)(2,1)S(1)}, u32[]{:S(2)}, u32[]{:S(2)}) async-start(bf16[8,24,1408]{2,1,0:T(8,128)(2,1)} %broadcast_in_dim.18), calls=%async_computation | async-start | bytes 1081344 | tf_op jit(solution)/shard_map/all_to_all | solution.py:23
  17.7 137.8 %all-gather.2.cloned.1.call-start = ((), (), s32[]{:S(2)}) async-start(), calls=%async_computation.8 | async-start | bytes 7028736 | tf_op jit(solution)/shard_map/all_gather | solution.py:152
  35.5 32.6 %copy-start.1 = (bf16[8,24,1408]{2,1,0:T(8,128)(2,1)}, bf16[8,24,1408]{2,1,0:T(8,128)(2,1)S(1)}, u32[]{:S(2)}) copy-start(bf16[8,24,1408]{2,1,0:T(8,128)(2,1)S(1)} %all-to-all-done) | copy-start | bytes 1622020
  68.6 1.7 copy-start.2
  70.3 12.4 %copy-start.3 = (bf16[512,512]{1,0:T(8,128)(2,1)S(1)}, bf16[512,512]{1,0:T(8,128)(2,1)}, u32[]{:S(2)}) copy-start(bf16[512,512]{1,0:T(8,128)(2,1)} %param.13) | copy-start | bytes 1572868
  82.7 33.8 %copy-start.4 = (f32[2,512]{1,0:T(2,128)S(1)}, f32[2,512]{1,0:T(2,128)}, u32[]{:S(2)}) copy-start(f32[2,512]{1,0:T(2,128)} %param.21) | copy-start | bytes 12292
  82.7 33.8 %copy-start.5 = (f32[2,512]{1,0:T(2,128)S(1)}, f32[2,512]{1,0:T(2,128)}, u32[]{:S(2)}) copy-start(f32[2,512]{1,0:T(2,128)} %param.20) | copy-start | bytes 12292
  82.7 33.8 %copy-start.6 = (f32[2,512]{1,0:T(2,128)S(1)}, f32[2,512]{1,0:T(2,128)}, u32[]{:S(2)}) copy-start(f32[2,512]{1,0:T(2,128)} %param.23) | copy-start | bytes 12292
  82.7 33.7 %copy-start.7 = (f32[2,512]{1,0:T(2,128)S(1)}, f32[2,512]{1,0:T(2,128)}, u32[]{:S(2)}) copy-start(f32[2,512]{1,0:T(2,128)} %param.22) | copy-start | bytes 12292
  146.2 8.7 %all-to-all-start.7 = ((f32[8,1,1024]{2,1,0:T(1,128)}), f32[8,1,1024]{2,1,0:T(1,128)S(1)}, u32[]{:S(2)}, u32[]{:S(2)}) async-start(f32[8,1,1024]{2,1,0:T(1,128)} %broadcast_in_dim.23), calls=%async_computation.7 | async-start | bytes 65536 | tf_op jit(solution)/shard_map/all_to_all | solution.py:23
Sparse Core Ops, SparseCore 0:
  68.2 78.9 all-gather.1

commit v5 on v4

--- a/solution.py
+++ b/solution.py
@@ -134,27 +134,28 @@
     columns = value_cot.shape[1]
     deep, high = lax.axis_size("fs_0"), lax.axis_size("fs_1")
 
-    piece = [w_value.astype(bf16), w_output.T.astype(bf16), proj_value, proj_output]
-    near = spread(jnp.concatenate(piece, axis=1), "fs_1")
-    near = near.reshape(-1, near.shape[-1])
     width = rank // lax.axis_size("tp")
     offset = lax.axis_index("tp") * width
-    at = 2 * columns
     own = jnp.concatenate(
         [
-            lax.dynamic_slice_in_dim(near[:, at : at + rank], offset, width, 1),
-            lax.dynamic_slice_in_dim(near[:, at + rank :], offset, width, 1),
+            lax.dynamic_slice_in_dim(proj_value, offset, width, 1),
+            lax.dynamic_slice_in_dim(proj_output, offset, width, 1),
         ],
         axis=1,
     )
-    rows = spread(own.T, "fs_0")
-    near, rows = lax.optimization_barrier((near, rows))
-    early = lax.all_gather(near, "fs_0", axis=0, tiled=True)
-    rows = jnp.swapaxes(rows, 0, 1).reshape(2 * width, -1)
+    share = spread(own.reshape(-1, proj_value.shape[0] * width), "fs_0")
+    share = share.reshape(-1, proj_value.shape[0] * width)
+    piece = [w_value.astype(bf16), w_output.T.astype(bf16), proj_value, proj_output, share]
+    near = spread(jnp.concatenate(piece, axis=1), "fs_1")
+    at = 2 * (columns + rank)
+    rows = near[:, :, at:].reshape(high, deep, -1, 2 * width)
+    rows = jnp.swapaxes(rows, 0, 1).reshape(-1, 2 * width)
+    early = lax.all_gather(near[:, :, :at].reshape(-1, at), "fs_0", axis=0, tiled=True)
+
     narrow = jnp.concatenate(
         [
-            contract(rows[:width], inputs, ((1,), (1,))),
-            contract(rows[width:], output_cot, ((1,), (1,))),
+            contract(rows[:, :width], inputs, ((0,), (1,))),
+            contract(rows[:, width:], output_cot, ((0,), (1,))),
         ],
         axis=0,
     ).astype(bf16)

time: 173 us -> 169 us (0.977)
  waiting for transfers between devices: 19.6 us -> 10.7 us
  starting transfers between devices: 12.5 us -> 20.5 us
  blocking collectives: 104 us -> 99.5 us
    all_to_all x2, waiting for transfers between devices: 19.6 us -> 10.7 us  [exchange(): return lax.all_to_all(pieces, axis, split_axis=0, concat_axis=0, tiled=True)]
    all_to_all x2, starting transfers between devices: 12.5 us -> 20.5 us  [exchange(): return lax.all_to_all(pieces, axis, split_axis=0, concat_axis=0, tiled=True)]
    all_to_all x6, blocking collectives: 104 us -> 99.5 us  [exchange(): return lax.all_to_all(pieces, axis, split_axis=0, concat_axis=0, tiled=True)]
  transfers between devices with their start and end apart: 3 -> 3, of which waited for: 2 -> 2; matrix products, arithmetic and copies ran while one was open for 5% -> 6% of each run, Pallas kernels for 0% -> 0%
where the time goes in v5:
time: 169 us; the launch traced here: 166 us
  blocking collectives  99.5 us (59%)
  starting transfers between devices  20.5 us (12%)
  between operations  14.3 us (8%)
  waiting for transfers between devices  10.7 us (6%)
  local copies, waits for them, and re-layouts  7.82 us (5%)
  Pallas kernels  7.12 us (4%)
  matrix products  3.39 us (2%)
  other arithmetic  2.58 us (2%)
    all_to_all x6, blocking collectives, exchange(): return lax.all_to_all(pieces, axis, split_axis=0, concat_axis=0, tiled=True)  99.5 us
    all_to_all x2, starting transfers between devices, exchange(): return lax.all_to_all(pieces, axis, split_axis=0, concat_axis=0, tiled=True)  20.5 us
    all_to_all x2, waiting for transfers between devices, exchange(): return lax.all_to_all(pieces, axis, split_axis=0, concat_axis=0, tiled=True)  10.7 us
    pallas_call x1, Pallas kernels, fold(): pl.pallas_call(functools.partial(fold_kernel, RANK * HV), grid=(rows // t...  7.12 us
    dot_general x4, matrix products, contract(): lax.dot_general(left, right, (dims, ((), ())), preferred_element_type=jnp...  3.39 us
  transfers between devices with their start and end apart: 3, of which 2 were waited for; matrix products, arithmetic and copies ran while one was open for 6% of the time, Pallas kernels for 0%

profile of v5, /device:TPU:6, one launch (start us, length us, event | category | flops | bytes accessed | tf_op | source)
XLA Modules:
  0.0 165.9 jit_solution(12843463232374573682)
XLA Ops:
  7.2 0.0 copy-start
  7.2 0.9 constant_dynamic-slice_fusion
  8.1 0.1 pad_maximum_fusion.2
  8.2 0.1 reshape.59
  8.3 0.6 broadcast_in_dim.18
  8.9 15.2 %all-to-all-start = ((bf16[12,2,576]{2,1,0:T(2,128)(2,1)}), bf16[12,2,576]{2,1,0:T(2,128)(2,1)S(1)}, u32[]{:S(2)}, u32[]{:S(2)}) async-start(bf16[12,2,576]{2,1,0:T(2,128)(2,1)} %broadcast_in_dim.18), calls=%async_computation | async-start | bytes 61440 | tf_op jit(solution)/shard_map/all_to_all | solution.py:23
  24.1 0.0 all-gather.2.cloned.1.call-start
  24.1 0.8 convert_bitcast_fusion
  25.0 0.8 convert_element_type.26
  25.8 8.9 %all-to-all-done = bf16[12,2,576]{2,1,0:T(2,128)(2,1)S(1)} async-done(((bf16[12,2,576]{2,1,0:T(2,128)(2,1)}), bf16[12,2,576]{2,1,0:T(2,128)(2,1)S(1)}, u32[]{:S(2)}, u32[]{:S(2)}) %all-to-all-start) | async-done | bytes 27680 | tf_op jit(solution)/shard_map/all_to_all | solution.py:23
  34.7 0.8 concatenate.19
  35.5 0.1 broadcast_in_dim.19
  35.6 28.6 %all_to_all.43 = bf16[8,24,1984]{2,1,0:T(8,128)(2,1)S(1)} all-to-all(bf16[8,24,1984]{2,1,0:T(8,128)(2,1)S(1)} %broadcast_in_dim.19), channel_id=1, replica_groups=mesh['fs_0'=12,'fs_1'=8,'tp'=8] {'fs_1'}, dimensions={0} | all-to-all | bytes 1523712 | tf_op jit(solution)/shard_map/all_to_all | solution.py:23
  64.1 0.8 slice.39
  65.0 0.0 all-gather.2.cloned.1.call-update
  65.1 0.5 reshape.61
  65.5 0.0 copy-start.1
  65.5 0.1 copy.33
  65.6 1.1 convolution_convert_fusion.2
  66.7 0.5 copy-done.1
  67.2 0.7 convolution_convert_fusion.3
  68.0 11.4 %all_to_all.44 = bf16[8,48,512]{2,1,0:T(8,128)(2,1)S(1)} all-to-all(bf16[8,48,512]{2,1,0:T(8,128)(2,1)S(1)} %broadcast_in_dim.20), channel_id=1, replica_groups=mesh['fs_0'=12,'fs_1'=8,'tp'=8] {'tp'}, dimensions={0} | all-to-all | bytes 786432 | tf_op jit(solution)/shard_map/all_to_all | solution.py:23
  79.4 0.1 dot_general.18
  79.5 0.1 dot_general.20
  79.6 0.0 copy-done.2
  79.6 0.0 copy-start.3
  79.6 0.0 copy-start.4
  79.6 0.0 copy-start.5
  79.7 0.0 copy-start.6
  79.7 0.3 convolution_convert_fusion.1
  79.9 1.3 convolution_convert_fusion
  81.3 0.2 copy.36
  81.5 17.2 %all_to_all.45 = bf16[8,24,1024]{2,1,0:T(8,128)(2,1)S(1)} all-to-all(bf16[8,24,1024]{2,1,0:T(8,128)(2,1)S(1)} %copy.36), channel_id=1, replica_groups=mesh['fs_0'=12,'fs_1'=8,'tp'=8] {'fs_1'}, dimensions={0} | all-to-all | bytes 786432 | tf_op jit(solution)/shard_map/all_to_all | solution.py:23
  98.7 0.1 reduce_sum.30
  98.8 14.0 %all_to_all.46 = bf16[12,2,1024]{2,1,0:T(2,128)(2,1)S(1)} all-to-all(bf16[12,2,1024]{2,1,0:T(2,128)(2,1)S(1)} %reshape.64), channel_id=1, replica_groups=mesh['fs_0'=12,'fs_1'=8,'tp'=8] {'fs_0'}, dimensions={0} | all-to-all | bytes 98304 | tf_op jit(solution)/shard_map/all_to_all | solution.py:23
  112.8 0.1 convert_reduce_fusion
  112.9 0.6 fusion.8
  113.6 14.0 %all_to_all.47 = bf16[12,2,1024]{2,1,0:T(2,128)(2,1)S(1)} all-to-all(bf16[12,2,1024]{2,1,0:T(2,128)(2,1)S(1)} %broadcast_in_dim.21), channel_id=1, replica_groups=mesh['fs_0'=12,'fs_1'=8,'tp'=8] {'fs_0'}, dimensions={0} | all-to-all | bytes 98304 | tf_op jit(solution)/shard_map/all_to_all | solution.py:23
  127.7 14.3 %all_to_all.48 = bf16[8,24,1024]{2,1,0:T(8,128)(2,1)S(1)} all-to-all(bf16[8,24,1024]{2,1,0:T(8,128)(2,1)S(1)} %broadcast_in_dim.22), channel_id=1, replica_groups=mesh['fs_0'=12,'fs_1'=8,'tp'=8] {'fs_1'}, dimensions={0} | all-to-all | bytes 786432 | tf_op jit(solution)/shard_map/all_to_all | solution.py:23
  141.9 0.1 multiply_reduce_fusion
  142.0 0.6 broadcast_in_dim.23
  142.7 5.3 %all-to-all-start.7 = ((f32[8,1,1024]{2,1,0:T(1,128)}), f32[8,1,1024]{2,1,0:T(1,128)S(1)}, u32[]{:S(2)}, u32[]{:S(2)}) async-start(f32[8,1,1024]{2,1,0:T(1,128)} %broadcast_in_dim.23), calls=%async_computation.7 | async-start | bytes 65536 | tf_op jit(solution)/shard_map/all_to_all | solution.py:23
  148.0 0.2 copy.37
  148.2 0.4 copy.38
  148.6 0.9 reshape.68.dirs_ref
  149.5 1.8 %all-to-all-done.7 = f32[8,1,1024]{2,1,0:T(1,128)S(1)} async-done(((f32[8,1,1024]{2,1,0:T(1,128)}), f32[8,1,1024]{2,1,0:T(1,128)S(1)}, u32[]{:S(2)}, u32[]{:S(2)}) %all-to-all-start.7) | async-done | bytes 32800 | tf_op jit(solution)/shard_map/all_to_all | solution.py:23
  151.3 0.6 copy.47
  152.0 7.1 %fold.1 = (bf16[2304,512]{1,0:T(8,128)(2,1)}, bf16[512,2304]{1,0:T(8,128)(2,1)}, f32[24,512]{1,0:T(8,128)}, f32[24,512]{1,0:T(8,128)}) custom-call(f32[8,1024]{1,0:T(8,128)} %bitcast.33, bf16[2304,1408]{1,0:T(8,128)(2,1)} %all-gather.2.cloned.1.call-done.early_ref, bf16[24,192]{1,0:T(8,128)(2,1)} %own_value_ref.1, bf16[24,192]{1,0:T(8,128)(2,1)} %own_output_ref.1, ...), custom_call_target="tpu_custom_call" | custom-call | tf_op jit(solution)/shard_map/fold/pallas_call | solution.py:91
  (18 shorter events, 0.3 us)
Async XLA Ops:
  7.2 58.5 %copy-start = (bf16[512,2304]{1,0:T(8,128)(2,1)S(1)}, bf16[512,2304]{1,0:T(8,128)(2,1)}, u32[]{:S(2)}) copy-start(bf16[512,2304]{1,0:T(8,128)(2,1)} %param.15) | copy-start | bytes 7077892
  8.9 25.7 %all-to-all-start = ((bf16[12,2,576]{2,1,0:T(2,128)(2,1)}), bf16[12,2,576]{2,1,0:T(2,128)(2,1)S(1)}, u32[]{:S(2)}, u32[]{:S(2)}) async-start(bf16[12,2,576]{2,1,0:T(2,128)(2,1)} %broadcast_in_dim.18), calls=%async_computation | async-start | bytes 61440 | tf_op jit(solution)/shard_map/all_to_all | solution.py:23
  24.1 127.9 %all-gather.2.cloned.1.call-start = ((), (), s32[]{:S(2)}) async-start(), calls=%async_computation.8 | async-start | bytes 7028736 | tf_op jit(solution)/shard_map/all_gather | solution.py:153
  65.5 1.7 %copy-start.1 = (bf16[512,2304]{1,0:T(8,128)(2,1)S(1)}, bf16[512,2304]{1,0:T(8,128)(2,1)}, u32[]{:S(2)}) copy-start(bf16[512,2304]{1,0:T(8,128)(2,1)} %param.12) | copy-start | bytes 7077892
  67.2 12.4 %copy-start.2 = (bf16[512,512]{1,0:T(8,128)(2,1)S(1)}, bf16[512,512]{1,0:T(8,128)(2,1)}, u32[]{:S(2)}) copy-start(bf16[512,512]{1,0:T(8,128)(2,1)} %param.13) | copy-start | bytes 1572868
  79.6 33.3 %copy-start.3 = (f32[2,512]{1,0:T(2,128)S(1)}, f32[2,512]{1,0:T(2,128)}, u32[]{:S(2)}) copy-start(f32[2,512]{1,0:T(2,128)} %param.21) | copy-start | bytes 12292
  79.6 33.3 %copy-start.4 = (f32[2,512]{1,0:T(2,128)S(1)}, f32[2,512]{1,0:T(2,128)}, u32[]{:S(2)}) copy-start(f32[2,512]{1,0:T(2,128)} %param.20) | copy-start | bytes 12292
  79.6 33.2 %copy-start.5 = (f32[2,512]{1,0:T(2,128)S(1)}, f32[2,512]{1,0:T(2,128)}, u32[]{:S(2)}) copy-start(f32[2,512]{1,0:T(2,128)} %param.23) | copy-start | bytes 12292
  79.7 33.2 %copy-start.6 = (f32[2,512]{1,0:T(2,128)S(1)}, f32[2,512]{1,0:T(2,128)}, u32[]{:S(2)}) copy-start(f32[2,512]{1,0:T(2,128)} %param.22) | copy-start | bytes 12292
  142.7 8.7 %all-to-all-start.7 = ((f32[8,1,1024]{2,1,0:T(1,128)}), f32[8,1,1024]{2,1,0:T(1,128)S(1)}, u32[]{:S(2)}, u32[]{:S(2)}) async-start(f32[8,1,1024]{2,1,0:T(1,128)} %broadcast_in_dim.23), calls=%async_computation.7 | async-start | bytes 65536 | tf_op jit(solution)/shard_map/all_to_all | solution.py:23
Sparse Core Ops, SparseCore 0:
  65.1 78.5 all-gather.1

commit v6 on v5

--- a/solution.py
+++ b/solution.py
@@ -146,7 +146,7 @@
     share = spread(own.reshape(-1, proj_value.shape[0] * width), "fs_0")
     share = share.reshape(-1, proj_value.shape[0] * width)
     piece = [w_value.astype(bf16), w_output.T.astype(bf16), proj_value, proj_output, share]
-    near = spread(jnp.concatenate(piece, axis=1), "fs_1")
+    near = lax.all_gather(jnp.concatenate(piece, axis=1), "fs_1")
     at = 2 * (columns + rank)
     rows = near[:, :, at:].reshape(high, deep, -1, 2 * width)
     rows = jnp.swapaxes(rows, 0, 1).reshape(-1, 2 * width)
@@ -176,7 +176,7 @@
     first_o, second_o, dir_output = adapt(first_output, second_output, summed[:, columns:])
 
     dirs = spread(jnp.concatenate([dir_value, dir_output], axis=1), "fs_0")
-    dirs = spread(dirs.reshape(-1, 2 * columns), "fs_1")
+    dirs = lax.all_gather(dirs.reshape(-1, 2 * columns), "fs_1")
     sums = jnp.square(dirs.astype(jnp.float32)).sum(axis=(0, 1))
     sums = spread(sums, "tp")
     dirs = dirs.reshape(high, deep, -1, 2 * columns)

time: 169 us -> 181 us (1.071)
  blocking collectives: 99.5 us -> 112 us
    all_gather x0 -> x2, blocking collectives: none -> 52.9 us  [the longest x1 27.8 us: per_device(): near = lax.all_gather(jnp.concatenate(piece, axis=1), 'fs_1')]
    all_to_all x6 -> x4, blocking collectives: 99.5 us -> 59.1 us  [exchange(): return lax.all_to_all(pieces, axis, split_axis=0, concat_axis=0, tiled=True)]
  transfers between devices with their start and end apart: 3 -> 3, of which waited for: 2 -> 2; matrix products, arithmetic and copies ran while one was open for 6% -> 5% of each run, Pallas kernels for 0% -> 0%
where the time goes in v6:
time: 181 us; the launch traced here: 178 us
  blocking collectives  112 us (62%)
  starting transfers between devices  20.6 us (11%)
  between operations  14.3 us (8%)
  waiting for transfers between devices  10.7 us (6%)
  local copies, waits for them, and re-layouts  7.71 us (4%)
  Pallas kernels  7.12 us (4%)
  matrix products  3.39 us (2%)
  other arithmetic  2.58 us (1%)
    all_to_all x4, blocking collectives, exchange(): return lax.all_to_all(pieces, axis, split_axis=0, concat_axis=0, tiled=True)  59.1 us
    all_gather x1, blocking collectives, per_device(): near = lax.all_gather(jnp.concatenate(piece, axis=1), 'fs_1')  27.8 us
    all_gather x1, blocking collectives, per_device(): dirs = lax.all_gather(dirs.reshape(-1, 2 * columns), 'fs_1')  25.1 us
    all_to_all x2, starting transfers between devices, exchange(): return lax.all_to_all(pieces, axis, split_axis=0, concat_axis=0, tiled=True)  20.5 us
    all_to_all x2, waiting for transfers between devices, exchange(): return lax.all_to_all(pieces, axis, split_axis=0, concat_axis=0, tiled=True)  10.7 us
    pallas_call x1, Pallas kernels, fold(): pl.pallas_call(functools.partial(fold_kernel, RANK * HV), grid=(rows // t...  7.12 us
  transfers between devices with their start and end apart: 3, of which 2 were waited for; matrix products, arithmetic and copies ran while one was open for 5% of the time, Pallas kernels for 0%

profile of v6, /device:TPU:6, one launch (start us, length us, event | category | flops | bytes accessed | tf_op | source)
XLA Modules:
  0.0 178.3 jit_solution(17024560245730820085)
XLA Ops:
  7.2 0.0 copy-start
  7.2 0.9 constant_dynamic-slice_fusion
  8.1 0.1 pad_maximum_fusion.2
  8.2 0.1 reshape.56
  8.3 0.6 broadcast_in_dim.12
  8.9 15.2 %all-to-all-start = ((bf16[12,2,576]{2,1,0:T(2,128)(2,1)}), bf16[12,2,576]{2,1,0:T(2,128)(2,1)S(1)}, u32[]{:S(2)}, u32[]{:S(2)}) async-start(bf16[12,2,576]{2,1,0:T(2,128)(2,1)} %broadcast_in_dim.12), calls=%async_computation | async-start | bytes 61440 | tf_op jit(solution)/shard_map/all_to_all | solution.py:23
  24.1 0.0 all-gather.3.cloned.1.call-start
  24.1 0.8 convert_bitcast_fusion
  25.0 0.8 convert_element_type.26
  25.8 8.9 %all-to-all-done = bf16[12,2,576]{2,1,0:T(2,128)(2,1)S(1)} async-done(((bf16[12,2,576]{2,1,0:T(2,128)(2,1)}), bf16[12,2,576]{2,1,0:T(2,128)(2,1)S(1)}, u32[]{:S(2)}, u32[]{:S(2)}) %all-to-all-start) | async-done | bytes 27680 | tf_op jit(solution)/shard_map/all_to_all | solution.py:23
  34.7 0.8 concatenate.19
  35.5 27.8 %all-gather = bf16[192,1984]{1,0:T(8,128)(2,1)S(1)} all-gather(bf16[24,1984]{1,0:T(8,128)(2,1)S(1)} %concatenate.19), channel_id=2, replica_groups=mesh['fs_0'=12,'fs_1'=8,'tp'=8] {'fs_1'}, dimensions={0}, use_global_device_ids=true | all-gather | bytes 857088 | tf_op jit(solution)/shard_map/all_gather | solution.py:149
  63.3 0.8 slice.39
  64.1 0.0 all-gather.3.cloned.1.call-update
  64.2 0.5 reshape.58
  64.7 0.0 copy-start.1
  64.7 0.1 copy.34
  64.8 0.0 copy-done
  64.8 1.1 convolution_convert_fusion.2
  65.9 0.5 copy-done.1
  66.3 0.7 convolution_convert_fusion.3
  67.1 11.4 %all_to_all.33 = bf16[8,48,512]{2,1,0:T(8,128)(2,1)S(1)} all-to-all(bf16[8,48,512]{2,1,0:T(8,128)(2,1)S(1)} %broadcast_in_dim.13), channel_id=1, replica_groups=mesh['fs_0'=12,'fs_1'=8,'tp'=8] {'tp'}, dimensions={0} | all-to-all | bytes 786432 | tf_op jit(solution)/shard_map/all_to_all | solution.py:23
  78.6 0.1 dot_general.18
  78.7 0.1 dot_general.20
  78.7 0.0 copy-done.2
  78.8 0.0 copy-start.3
  78.8 0.0 copy-start.4
  78.8 0.0 copy-start.5
  78.8 0.0 copy-start.6
  78.8 0.3 convolution_convert_fusion.1
  79.1 1.3 convolution_convert_fusion
  80.4 0.2 copy.37
  80.7 19.7 %all_to_all.34 = bf16[8,24,1024]{2,1,0:T(8,128)(2,1)S(1)} all-to-all(bf16[8,24,1024]{2,1,0:T(8,128)(2,1)S(1)} %copy.37), channel_id=1, replica_groups=mesh['fs_0'=12,'fs_1'=8,'tp'=8] {'fs_1'}, dimensions={0} | all-to-all | bytes 786432 | tf_op jit(solution)/shard_map/all_to_all | solution.py:23
  100.3 0.1 reduce_sum.30
  100.4 14.0 %all_to_all.35 = bf16[12,2,1024]{2,1,0:T(2,128)(2,1)S(1)} all-to-all(bf16[12,2,1024]{2,1,0:T(2,128)(2,1)S(1)} %reshape.61), channel_id=1, replica_groups=mesh['fs_0'=12,'fs_1'=8,'tp'=8] {'fs_0'}, dimensions={0} | all-to-all | bytes 98304 | tf_op jit(solution)/shard_map/all_to_all | solution.py:23
  114.4 0.1 convert_reduce_fusion
  114.5 0.6 fusion.8
  115.2 14.0 %all_to_all.36 = bf16[12,2,1024]{2,1,0:T(2,128)(2,1)S(1)} all-to-all(bf16[12,2,1024]{2,1,0:T(2,128)(2,1)S(1)} %broadcast_in_dim.14), channel_id=1, replica_groups=mesh['fs_0'=12,'fs_1'=8,'tp'=8] {'fs_0'}, dimensions={0} | all-to-all | bytes 98304 | tf_op jit(solution)/shard_map/all_to_all | solution.py:23
  129.2 25.1 %all_gather.14 = bf16[8,24,1024]{2,1,0:T(8,128)(2,1)S(1)} all-gather(bf16[1,24,1024]{2,1,0:T(8,128)(2,1)S(1)} %all_gather_reshape.3), channel_id=1, replica_groups=mesh['fs_0'=12,'fs_1'=8,'tp'=8] {'fs_1'}, dimensions={0}, use_global_device_ids=true | all-gather | bytes 442368 | tf_op jit(solution)/shard_map/all_gather | solution.py:179
  154.3 0.1 multiply_reduce_fusion
  154.4 0.6 broadcast_in_dim.15
  155.0 5.4 %all-to-all-start.5 = ((f32[8,1,1024]{2,1,0:T(1,128)}), f32[8,1,1024]{2,1,0:T(1,128)S(1)}, u32[]{:S(2)}, u32[]{:S(2)}) async-start(f32[8,1,1024]{2,1,0:T(1,128)} %broadcast_in_dim.15), calls=%async_computation.5 | async-start | bytes 65536 | tf_op jit(solution)/shard_map/all_to_all | solution.py:23
  160.4 0.2 copy.38
  160.6 0.4 copy.39
  161.0 0.9 reshape.64.dirs_ref
  161.9 1.8 %all-to-all-done.5 = f32[8,1,1024]{2,1,0:T(1,128)S(1)} async-done(((f32[8,1,1024]{2,1,0:T(1,128)}), f32[8,1,1024]{2,1,0:T(1,128)S(1)}, u32[]{:S(2)}, u32[]{:S(2)}) %all-to-all-start.5) | async-done | bytes 32800 | tf_op jit(solution)/shard_map/all_to_all | solution.py:23
  163.7 0.6 copy.48
  164.4 7.1 %fold.1 = (bf16[2304,512]{1,0:T(8,128)(2,1)}, bf16[512,2304]{1,0:T(8,128)(2,1)}, f32[24,512]{1,0:T(8,128)}, f32[24,512]{1,0:T(8,128)}) custom-call(f32[8,1024]{1,0:T(8,128)} %bitcast.36, bf16[2304,1408]{1,0:T(8,128)(2,1)} %all-gather.3.cloned.1.call-done.early_ref, bf16[24,192]{1,0:T(8,128)(2,1)} %own_value_ref.1, bf16[24,192]{1,0:T(8,128)(2,1)} %own_output_ref.1, ...), custom_call_target="tpu_custom_call" | custom-call | tf_op jit(solution)/shard_map/fold/pallas_call | solution.py:91
  (16 shorter events, 0.3 us)
Async XLA Ops:
  7.2 57.6 %copy-start = (bf16[512,2304]{1,0:T(8,128)(2,1)S(1)}, bf16[512,2304]{1,0:T(8,128)(2,1)}, u32[]{:S(2)}) copy-start(bf16[512,2304]{1,0:T(8,128)(2,1)} %param.15) | copy-start | bytes 7077892
  8.9 25.7 %all-to-all-start = ((bf16[12,2,576]{2,1,0:T(2,128)(2,1)}), bf16[12,2,576]{2,1,0:T(2,128)(2,1)S(1)}, u32[]{:S(2)}, u32[]{:S(2)}) async-start(bf16[12,2,576]{2,1,0:T(2,128)(2,1)} %broadcast_in_dim.12), calls=%async_computation | async-start | bytes 61440 | tf_op jit(solution)/shard_map/all_to_all | solution.py:23
  24.1 140.3 %all-gather.3.cloned.1.call-start = ((), (), s32[]{:S(2)}) async-start(), calls=%async_computation.6 | async-start | bytes 7028736 | tf_op jit(solution)/shard_map/all_gather | solution.py:153
  64.7 1.7 copy-start.1
  66.3 12.4 %copy-start.2 = (bf16[512,512]{1,0:T(8,128)(2,1)S(1)}, bf16[512,512]{1,0:T(8,128)(2,1)}, u32[]{:S(2)}) copy-start(bf16[512,512]{1,0:T(8,128)(2,1)} %param.13) | copy-start | bytes 1572868
  78.8 35.7 %copy-start.3 = (f32[2,512]{1,0:T(2,128)S(1)}, f32[2,512]{1,0:T(2,128)}, u32[]{:S(2)}) copy-start(f32[2,512]{1,0:T(2,128)} %param.21) | copy-start | bytes 12292
  78.8 35.7 %copy-start.4 = (f32[2,512]{1,0:T(2,128)S(1)}, f32[2,512]{1,0:T(2,128)}, u32[]{:S(2)}) copy-start(f32[2,512]{1,0:T(2,128)} %param.20) | copy-start | bytes 12292
  78.8 35.7 %copy-start.5 = (f32[2,512]{1,0:T(2,128)S(1)}, f32[2,512]{1,0:T(2,128)}, u32[]{:S(2)}) copy-start(f32[2,512]{1,0:T(2,128)} %param.23) | copy-start | bytes 12292
  78.8 35.7 %copy-start.6 = (f32[2,512]{1,0:T(2,128)S(1)}, f32[2,512]{1,0:T(2,128)}, u32[]{:S(2)}) copy-start(f32[2,512]{1,0:T(2,128)} %param.22) | copy-start | bytes 12292
  155.0 8.7 %all-to-all-start.5 = ((f32[8,1,1024]{2,1,0:T(1,128)}), f32[8,1,1024]{2,1,0:T(1,128)S(1)}, u32[]{:S(2)}, u32[]{:S(2)}) async-start(f32[8,1,1024]{2,1,0:T(1,128)} %broadcast_in_dim.15), calls=%async_computation.5 | async-start | bytes 65536 | tf_op jit(solution)/shard_map/all_to_all | solution.py:23
Sparse Core Ops, SparseCore 0:
  64.3 81.6 all-gather.2

commit v7 on v5

--- a/solution.py
+++ b/solution.py
@@ -143,15 +143,10 @@
         ],
         axis=1,
     )
-    share = spread(own.reshape(-1, proj_value.shape[0] * width), "fs_0")
-    share = share.reshape(-1, proj_value.shape[0] * width)
-    piece = [w_value.astype(bf16), w_output.T.astype(bf16), proj_value, proj_output, share]
-    near = spread(jnp.concatenate(piece, axis=1), "fs_1")
-    at = 2 * (columns + rank)
-    rows = near[:, :, at:].reshape(high, deep, -1, 2 * width)
-    rows = jnp.swapaxes(rows, 0, 1).reshape(-1, 2 * width)
-    early = lax.all_gather(near[:, :, :at].reshape(-1, at), "fs_0", axis=0, tiled=True)
-
+    rows = spread(own.reshape(-1, proj_value.shape[0] * width), FS).reshape(-1, 2 * width)
+    piece = [w_value.astype(bf16), w_output.T.astype(bf16), proj_value, proj_output]
+    piece, rows = lax.optimization_barrier((jnp.concatenate(piece, axis=1), rows))
+    near = spread(piece, "fs_1")
     narrow = jnp.concatenate(
         [
             contract(rows[:, :width], inputs, ((0,), (1,))),
@@ -159,6 +154,9 @@
         ],
         axis=0,
     ).astype(bf16)
+    near, narrow = lax.optimization_barrier((near, narrow))
+    early = lax.all_gather(near.reshape(-1, near.shape[-1]), "fs_0", axis=0, tiled=True)
+
     projected = spread(narrow, "tp")
     x_proj = projected[:, :width].reshape(rank, -1)
     o_proj = projected[:, width:].reshape(rank, -1)

time: 169 us -> 174 us (1.030)
  blocking collectives: 99.5 us -> 71.8 us
  waiting for transfers between devices: 10.7 us -> 32 us
  starting transfers between devices: 20.5 us -> 31 us
    all_to_all x6 -> x5, blocking collectives: 99.5 us -> 71.8 us  [exchange(): return lax.all_to_all(pieces, axis, split_axis=0, concat_axis=0, tiled=True)]
    all_to_all x2 -> x3, waiting for transfers between devices: 10.7 us -> 32 us  [exchange(): return lax.all_to_all(pieces, axis, split_axis=0, concat_axis=0, tiled=True)]
    all_to_all x2 -> x3, starting transfers between devices: 20.5 us -> 30.9 us  [exchange(): return lax.all_to_all(pieces, axis, split_axis=0, concat_axis=0, tiled=True)]
  transfers between devices with their start and end apart: 3 -> 4, of which waited for: 2 -> 3; matrix products, arithmetic and copies ran while one was open for 6% -> 6% of each run, Pallas kernels for 0% -> 0%
where the time goes in v7:
time: 174 us; the launch traced here: 171 us
  blocking collectives  71.8 us (41%)
  waiting for transfers between devices  32 us (18%)
  starting transfers between devices  31 us (18%)
  between operations  14.3 us (8%)
  local copies, waits for them, and re-layouts  8.98 us (5%)
  Pallas kernels  7.13 us (4%)
  matrix products  3.39 us (2%)
  other arithmetic  2.57 us (1%)
    all_to_all x5, blocking collectives, exchange(): return lax.all_to_all(pieces, axis, split_axis=0, concat_axis=0, tiled=True)  71.8 us
    all_to_all x3, waiting for transfers between devices, exchange(): return lax.all_to_all(pieces, axis, split_axis=0, concat_axis=0, tiled=True)  32 us
    all_to_all x3, starting transfers between devices, exchange(): return lax.all_to_all(pieces, axis, split_axis=0, concat_axis=0, tiled=True)  30.9 us
    pallas_call x1, Pallas kernels, fold(): pl.pallas_call(functools.partial(fold_kernel, RANK * HV), grid=(rows // t...  7.13 us
  transfers between devices with their start and end apart: 4, of which 3 were waited for; matrix products, arithmetic and copies ran while one was open for 6% of the time, Pallas kernels for 0%

profile of v7, /device:TPU:6, one launch (start us, length us, event | category | flops | bytes accessed | tf_op | source)
XLA Modules:
  0.0 171.2 jit_solution(17247402315497870820)
XLA Ops:
  7.2 0.0 copy-start
  7.2 0.9 constant_dynamic-slice_fusion
  8.1 0.1 pad_maximum_fusion.2
  8.2 0.1 reshape.53
  8.3 0.8 broadcast_in_dim.18
  9.1 22.0 %all-to-all-start = ((bf16[96,2,576]{2,1,0:T(2,128)(2,1)}), bf16[96,2,576]{2,1,0:T(2,128)(2,1)S(1)}, u32[]{:S(2)}, u32[]{:S(2)}) async-start(bf16[96,2,576]{2,1,0:T(2,128)(2,1)} %broadcast_in_dim.18), calls=%async_computation | async-start | bytes 491520 | tf_op jit(solution)/shard_map/all_to_all | solution.py:23
  31.1 0.8 convert_element_type.26
  31.9 0.8 convert_bitcast_fusion
  32.7 0.8 concatenate.18
  33.6 16.9 %all-to-all-done = bf16[96,2,576]{2,1,0:T(2,128)(2,1)S(1)} async-done(((bf16[96,2,576]{2,1,0:T(2,128)(2,1)}), bf16[96,2,576]{2,1,0:T(2,128)(2,1)S(1)}, u32[]{:S(2)}, u32[]{:S(2)}) %all-to-all-start) | async-done | bytes 221216 | tf_op jit(solution)/shard_map/all_to_all | solution.py:23
  50.5 0.7 reshape.54
  51.2 0.8 broadcast_in_dim.19
  52.0 3.5 %all-to-all-start.1 = ((bf16[8,24,1408]{2,1,0:T(8,128)(2,1)}), bf16[8,24,1408]{2,1,0:T(8,128)(2,1)S(1)}, u32[]{:S(2)}, u32[]{:S(2)}) async-start(bf16[8,24,1408]{2,1,0:T(8,128)(2,1)} %broadcast_in_dim.19), calls=%async_computation.1 | async-start | bytes 1081344 | tf_op jit(solution)/shard_map/all_to_all | solution.py:23
  55.6 0.0 all-gather.2.cloned.1.call-start
  55.6 0.0 copy-start.1
  55.6 1.1 convolution_convert_fusion.2
  56.7 0.6 copy-done.1
  57.3 0.7 convolution_convert_fusion.3
  58.0 13.3 %all-to-all-done.1 = bf16[8,24,1408]{2,1,0:T(8,128)(2,1)S(1)} async-done(((bf16[8,24,1408]{2,1,0:T(8,128)(2,1)}), bf16[8,24,1408]{2,1,0:T(8,128)(2,1)S(1)}, u32[]{:S(2)}, u32[]{:S(2)}) %all-to-all-start.1) | async-done | bytes 540704 | tf_op jit(solution)/shard_map/all_to_all | solution.py:23
  71.3 0.8 copy-done.2
  72.1 0.0 all-gather.2.cloned.1.call-update
  72.2 11.4 %all_to_all.43 = bf16[8,48,512]{2,1,0:T(8,128)(2,1)S(1)} all-to-all(bf16[8,48,512]{2,1,0:T(8,128)(2,1)S(1)} %broadcast_in_dim.20), channel_id=1, replica_groups=mesh['fs_0'=12,'fs_1'=8,'tp'=8] {'tp'}, dimensions={0} | all-to-all | bytes 786432 | tf_op jit(solution)/shard_map/all_to_all | solution.py:23
  83.7 0.1 dot_general.18
  83.7 0.1 dot_general.20
  83.8 0.0 copy-start.4
  83.9 0.0 copy-start.5
  83.9 0.0 copy-start.6
  83.9 0.0 copy-start.7
  83.9 0.3 convolution_convert_fusion.1
  84.2 1.3 convolution_convert_fusion
  85.5 0.2 copy.30
  85.8 17.2 %all_to_all.44 = bf16[8,24,1024]{2,1,0:T(8,128)(2,1)S(1)} all-to-all(bf16[8,24,1024]{2,1,0:T(8,128)(2,1)S(1)} %copy.30), channel_id=1, replica_groups=mesh['fs_0'=12,'fs_1'=8,'tp'=8] {'fs_1'}, dimensions={0} | all-to-all | bytes 786432 | tf_op jit(solution)/shard_map/all_to_all | solution.py:23
  102.9 0.1 reduce_sum.30
  103.0 15.0 %all_to_all.45 = bf16[12,2,1024]{2,1,0:T(2,128)(2,1)S(1)} all-to-all(bf16[12,2,1024]{2,1,0:T(2,128)(2,1)S(1)} %reshape.56), channel_id=1, replica_groups=mesh['fs_0'=12,'fs_1'=8,'tp'=8] {'fs_0'}, dimensions={0} | all-to-all | bytes 98304 | tf_op jit(solution)/shard_map/all_to_all | solution.py:23
  118.0 0.1 convert_reduce_fusion
  118.0 0.0 copy-done.4
  118.1 0.6 fusion.8
  118.7 14.0 %all_to_all.46 = bf16[12,2,1024]{2,1,0:T(2,128)(2,1)S(1)} all-to-all(bf16[12,2,1024]{2,1,0:T(2,128)(2,1)S(1)} %broadcast_in_dim.21), channel_id=1, replica_groups=mesh['fs_0'=12,'fs_1'=8,'tp'=8] {'fs_0'}, dimensions={0} | all-to-all | bytes 98304 | tf_op jit(solution)/shard_map/all_to_all | solution.py:23
  132.8 14.3 %all_to_all.47 = bf16[8,24,1024]{2,1,0:T(8,128)(2,1)S(1)} all-to-all(bf16[8,24,1024]{2,1,0:T(8,128)(2,1)S(1)} %broadcast_in_dim.22), channel_id=1, replica_groups=mesh['fs_0'=12,'fs_1'=8,'tp'=8] {'fs_1'}, dimensions={0} | all-to-all | bytes 786432 | tf_op jit(solution)/shard_map/all_to_all | solution.py:23
  147.1 0.1 multiply_reduce_fusion
  147.2 0.6 broadcast_in_dim.23
  147.8 5.4 %all-to-all-start.7 = ((f32[8,1,1024]{2,1,0:T(1,128)}), f32[8,1,1024]{2,1,0:T(1,128)S(1)}, u32[]{:S(2)}, u32[]{:S(2)}) async-start(f32[8,1,1024]{2,1,0:T(1,128)} %broadcast_in_dim.23), calls=%async_computation.7 | async-start | bytes 65536 | tf_op jit(solution)/shard_map/all_to_all | solution.py:23
  153.2 0.2 copy.31
  153.4 0.4 copy.32
  153.8 0.9 reshape.60.dirs_ref
  154.8 1.8 %all-to-all-done.7 = f32[8,1,1024]{2,1,0:T(1,128)S(1)} async-done(((f32[8,1,1024]{2,1,0:T(1,128)}), f32[8,1,1024]{2,1,0:T(1,128)S(1)}, u32[]{:S(2)}, u32[]{:S(2)}) %all-to-all-start.7) | async-done | bytes 32800 | tf_op jit(solution)/shard_map/all_to_all | solution.py:23
  156.6 0.6 copy.41
  157.2 7.1 %fold.1 = (bf16[2304,512]{1,0:T(8,128)(2,1)}, bf16[512,2304]{1,0:T(8,128)(2,1)}, f32[24,512]{1,0:T(8,128)}, f32[24,512]{1,0:T(8,128)}) custom-call(f32[8,1024]{1,0:T(8,128)} %bitcast.28, bf16[2304,1408]{1,0:T(8,128)(2,1)} %all-gather.2.cloned.1.call-done.early_ref, bf16[24,192]{1,0:T(8,128)(2,1)} %own_value_ref.1, bf16[24,192]{1,0:T(8,128)(2,1)} %own_output_ref.1, ...), custom_call_target="tpu_custom_call" | custom-call | tf_op jit(solution)/shard_map/fold/pallas_call | solution.py:91
  (17 shorter events, 0.2 us)
Async XLA Ops:
  7.2 48.4 %copy-start = (bf16[512,2304]{1,0:T(8,128)(2,1)S(1)}, bf16[512,2304]{1,0:T(8,128)(2,1)}, u32[]{:S(2)}) copy-start(bf16[512,2304]{1,0:T(8,128)(2,1)} %param.15) | copy-start | bytes 7077892
  9.1 41.3 %all-to-all-start = ((bf16[96,2,576]{2,1,0:T(2,128)(2,1)}), bf16[96,2,576]{2,1,0:T(2,128)(2,1)S(1)}, u32[]{:S(2)}, u32[]{:S(2)}) async-start(bf16[96,2,576]{2,1,0:T(2,128)(2,1)} %broadcast_in_dim.18), calls=%async_computation | async-start | bytes 491520 | tf_op jit(solution)/shard_map/all_to_all | solution.py:23
  52.0 19.3 %all-to-all-start.1 = ((bf16[8,24,1408]{2,1,0:T(8,128)(2,1)}), bf16[8,24,1408]{2,1,0:T(8,128)(2,1)S(1)}, u32[]{:S(2)}, u32[]{:S(2)}) async-start(bf16[8,24,1408]{2,1,0:T(8,128)(2,1)} %broadcast_in_dim.19), calls=%async_computation.1 | async-start | bytes 1081344 | tf_op jit(solution)/shard_map/all_to_all | solution.py:23
  55.6 101.6 %all-gather.2.cloned.1.call-start = ((), (), s32[]{:S(2)}) async-start(), calls=%async_computation.8 | async-start | bytes 7028736 | tf_op jit(solution)/shard_map/all_gather | solution.py:158
  55.6 1.7 copy-start.1
  58.0 25.8 %copy-start.3 = (bf16[512,512]{1,0:T(8,128)(2,1)S(1)}, bf16[512,512]{1,0:T(8,128)(2,1)}, u32[]{:S(2)}) copy-start(bf16[512,512]{1,0:T(8,128)(2,1)} %param.13) | copy-start | bytes 1572868
  71.3 0.8 copy-start.2
  83.8 34.2 %copy-start.4 = (f32[2,512]{1,0:T(2,128)S(1)}, f32[2,512]{1,0:T(2,128)}, u32[]{:S(2)}) copy-start(f32[2,512]{1,0:T(2,128)} %param.21) | copy-start | bytes 12292
  83.9 34.2 %copy-start.5 = (f32[2,512]{1,0:T(2,128)S(1)}, f32[2,512]{1,0:T(2,128)}, u32[]{:S(2)}) copy-start(f32[2,512]{1,0:T(2,128)} %param.20) | copy-start | bytes 12292
  83.9 34.2 %copy-start.6 = (f32[2,512]{1,0:T(2,128)S(1)}, f32[2,512]{1,0:T(2,128)}, u32[]{:S(2)}) copy-start(f32[2,512]{1,0:T(2,128)} %param.23) | copy-start | bytes 12292
  83.9 34.2 %copy-start.7 = (f32[2,512]{1,0:T(2,128)S(1)}, f32[2,512]{1,0:T(2,128)}, u32[]{:S(2)}) copy-start(f32[2,512]{1,0:T(2,128)} %param.22) | copy-start | bytes 12292
  147.8 8.8 %all-to-all-start.7 = ((f32[8,1,1024]{2,1,0:T(1,128)}), f32[8,1,1024]{2,1,0:T(1,128)S(1)}, u32[]{:S(2)}, u32[]{:S(2)}) async-start(f32[8,1,1024]{2,1,0:T(1,128)} %broadcast_in_dim.23), calls=%async_computation.7 | async-start | bytes 65536 | tf_op jit(solution)/shard_map/all_to_all | solution.py:23
Sparse Core Ops, SparseCore 0:
  72.3 79.5 all-gather.1

commit v8 on v5

--- a/solution.py
+++ b/solution.py
@@ -54,11 +54,13 @@
     at = 2 * columns
 
     def scale_of(sums):
-        total = jnp.sum(jnp.sum(sums, axis=1, keepdims=True), axis=0, keepdims=True)
+        total = jnp.sum(sums, axis=0)
+        total = jnp.sum(jnp.sum(total, axis=1, keepdims=True), axis=0, keepdims=True)
         return lax.rsqrt(total / count + norm_eps)
 
-    scale_value = scale_of(sums_ref[:, :columns])
-    scale_output = scale_of(sums_ref[:, columns:])
+    half = sums_ref.shape[1] // 2
+    scale_value = scale_of(sums_ref[:, :half])
+    scale_output = scale_of(sums_ref[:, half:])
 
     @pl.when(pl.program_id(0) == 0)
     def _():
@@ -92,7 +94,7 @@
         functools.partial(fold_kernel, RANK * HV),
         grid=(rows // tile,),
         in_specs=[
-            whole(*sums.shape),
+            pl.BlockSpec(sums.shape, lambda i: (0, 0, 0)),
             pl.BlockSpec((tile, early.shape[1]), lambda i: (i, 0)),
             whole(own, rank),
             whole(own, rank),
@@ -134,6 +136,9 @@
     columns = value_cot.shape[1]
     deep, high = lax.axis_size("fs_0"), lax.axis_size("fs_1")
 
+    piece = [w_value.astype(bf16), w_output.T.astype(bf16), proj_value, proj_output]
+    early = lax.all_gather(jnp.concatenate(piece, axis=1), FS, axis=0, tiled=True)
+
     width = rank // lax.axis_size("tp")
     offset = lax.axis_index("tp") * width
     own = jnp.concatenate(
@@ -144,13 +149,9 @@
         axis=1,
     )
     share = spread(own.reshape(-1, proj_value.shape[0] * width), "fs_0")
-    share = share.reshape(-1, proj_value.shape[0] * width)
-    piece = [w_value.astype(bf16), w_output.T.astype(bf16), proj_value, proj_output, share]
-    near = spread(jnp.concatenate(piece, axis=1), "fs_1")
-    at = 2 * (columns + rank)
-    rows = near[:, :, at:].reshape(high, deep, -1, 2 * width)
+    share = spread(share.reshape(-1, proj_value.shape[0] * width), "fs_1")
+    rows = share.reshape(high, deep, -1, 2 * width)
     rows = jnp.swapaxes(rows, 0, 1).reshape(-1, 2 * width)
-    early = lax.all_gather(near[:, :, :at].reshape(-1, at), "fs_0", axis=0, tiled=True)
 
     narrow = jnp.concatenate(
         [
@@ -178,7 +179,7 @@
     dirs = spread(jnp.concatenate([dir_value, dir_output], axis=1), "fs_0")
     dirs = spread(dirs.reshape(-1, 2 * columns), "fs_1")
     sums = jnp.square(dirs.astype(jnp.float32)).sum(axis=(0, 1))
-    sums = spread(sums, "tp")
+    sums = spread(sums.reshape(-1, 128), "tp")
     dirs = dirs.reshape(high, deep, -1, 2 * columns)
     dirs = jnp.swapaxes(dirs, 0, 1).reshape(rank, -1)
 

time: 169 us -> 171 us (1.012); the launches traced: 166 us -> 171 us
  blocking collectives: 99.5 us -> 118 us
  starting transfers between devices: 20.5 us -> 4.98 us
  waiting for transfers between devices: 10.7 us -> 13.8 us
    all_to_all x6 -> x7, blocking collectives: 99.5 us -> 118 us  [exchange(): return lax.all_to_all(pieces, axis, split_axis=0, concat_axis=0, tiled=True)]
    all_to_all x2 -> x1, starting transfers between devices: 20.5 us -> 4.94 us  [exchange(): return lax.all_to_all(pieces, axis, split_axis=0, concat_axis=0, tiled=True)]
    all_gather x1, waiting for transfers between devices: 0.01 us -> 12 us  [per_device(): lax.all_gather(jnp.concatenate(piece, axis=1), FS, axis=0, tiled=True)]
    all_to_all x2 -> x1, waiting for transfers between devices: 10.7 us -> 1.81 us  [exchange(): return lax.all_to_all(pieces, axis, split_axis=0, concat_axis=0, tiled=True)]
  transfers between devices with their start and end apart: 3 -> 2, of which waited for: 2 -> 2; matrix products, arithmetic and copies ran while one was open for 6% -> 5% of each run, Pallas kernels for 0% -> 0%
where the time goes in v8:
time: 171 us
  blocking collectives  118 us (69%)
  between operations  14.3 us (8%)
  waiting for transfers between devices  13.8 us (8%)
  Pallas kernels  6.75 us (4%)
  local copies, waits for them, and re-layouts  6.14 us (4%)
  starting transfers between devices  4.98 us (3%)
  matrix products  3.39 us (2%)
  other arithmetic  2.72 us (2%)
    all_to_all x7, blocking collectives, exchange(): return lax.all_to_all(pieces, axis, split_axis=0, concat_axis=0, tiled=True)  118 us
    all_gather x1, waiting for transfers between devices, per_device(): lax.all_gather(jnp.concatenate(piece, axis=1), FS, axis=0, tiled=True)  12 us
    pallas_call x1, Pallas kernels, fold(): pl.pallas_call(functools.partial(fold_kernel, RANK * HV), grid=(rows // t...  6.75 us
    all_to_all x1, starting transfers between devices, exchange(): return lax.all_to_all(pieces, axis, split_axis=0, concat_axis=0, tiled=True)  4.94 us
  transfers between devices with their start and end apart: 2, of which 2 were waited for; matrix products, arithmetic and copies ran while one was open for 5% of the time, Pallas kernels for 0%

profile of v8, /device:TPU:6, one launch (start us, length us, event | category | flops | bytes accessed | tf_op | source)
XLA Modules:
  0.0 170.5 jit_solution(4912409475327945911)
XLA Ops:
  7.2 0.0 copy-start
  7.2 0.0 all-gather.2.cloned.1.call-start
  7.2 1.0 convert_element_type.30
  8.2 0.8 convert_bitcast_fusion
  9.0 1.4 concatenate.22
  10.4 0.0 all-gather.2.cloned.1.call-update
  10.5 0.8 constant_dynamic-slice_fusion
  11.3 0.1 pad_maximum_fusion.2
  11.3 0.1 reshape.55
  11.5 25.5 %all_to_all.40 = bf16[12,2,576]{2,1,0:T(2,128)(2,1)S(1)} all-to-all(bf16[12,2,576]{2,1,0:T(2,128)(2,1)S(1)} %broadcast_in_dim.18), channel_id=1, replica_groups=mesh['fs_0'=12,'fs_1'=8,'tp'=8] {'fs_0'}, dimensions={0} | all-to-all | bytes 55296 | tf_op jit(solution)/shard_map/all_to_all | solution.py:23
  37.0 17.5 %all_to_all.41 = bf16[8,24,576]{2,1,0:T(8,128)(2,1)S(1)} all-to-all(bf16[8,24,576]{2,1,0:T(8,128)(2,1)S(1)} %broadcast_in_dim.19), channel_id=1, replica_groups=mesh['fs_0'=12,'fs_1'=8,'tp'=8] {'fs_1'}, dimensions={0} | all-to-all | bytes 442368 | tf_op jit(solution)/shard_map/all_to_all | solution.py:23
  54.5 0.5 reshape.57
  55.0 0.0 copy-start.1
  55.0 0.1 copy.33
  55.1 0.0 copy-done
  55.1 1.1 convolution_convert_fusion.2
  56.2 0.4 copy-done.1
  56.7 0.7 convolution_convert_fusion.3
  57.5 11.4 %all_to_all.42 = bf16[8,48,512]{2,1,0:T(8,128)(2,1)S(1)} all-to-all(bf16[8,48,512]{2,1,0:T(8,128)(2,1)S(1)} %broadcast_in_dim.20), channel_id=1, replica_groups=mesh['fs_0'=12,'fs_1'=8,'tp'=8] {'tp'}, dimensions={0} | all-to-all | bytes 786432 | tf_op jit(solution)/shard_map/all_to_all | solution.py:23
  68.9 0.1 dot_general.18
  69.0 0.1 dot_general.20
  69.1 0.0 copy-done.2
  69.1 0.0 copy-start.4
  69.1 0.0 copy-start.5
  69.1 0.0 copy-start.6
  69.1 0.0 copy-start.7
  69.2 0.3 convolution_convert_fusion.1
  69.4 1.3 convolution_convert_fusion
  70.8 0.2 copy.36
  71.0 17.2 %all_to_all.43 = bf16[8,24,1024]{2,1,0:T(8,128)(2,1)S(1)} all-to-all(bf16[8,24,1024]{2,1,0:T(8,128)(2,1)S(1)} %copy.36), channel_id=1, replica_groups=mesh['fs_0'=12,'fs_1'=8,'tp'=8] {'fs_1'}, dimensions={0} | all-to-all | bytes 786432 | tf_op jit(solution)/shard_map/all_to_all | solution.py:23
  88.2 0.1 reduce_sum.30
  88.3 13.5 %all_to_all.44 = bf16[12,2,1024]{2,1,0:T(2,128)(2,1)S(1)} all-to-all(bf16[12,2,1024]{2,1,0:T(2,128)(2,1)S(1)} %reshape.60), channel_id=1, replica_groups=mesh['fs_0'=12,'fs_1'=8,'tp'=8] {'fs_0'}, dimensions={0} | all-to-all | bytes 98304 | tf_op jit(solution)/shard_map/all_to_all | solution.py:23
  101.8 0.1 convert_reduce_fusion
  101.9 0.0 copy-done.4
  101.9 0.0 copy-done.5
  101.9 0.0 copy-done.6
  101.9 0.6 fusion.8
  102.6 13.7 %all_to_all.45 = bf16[12,2,1024]{2,1,0:T(2,128)(2,1)S(1)} all-to-all(bf16[12,2,1024]{2,1,0:T(2,128)(2,1)S(1)} %broadcast_in_dim.21), channel_id=1, replica_groups=mesh['fs_0'=12,'fs_1'=8,'tp'=8] {'fs_0'}, dimensions={0} | all-to-all | bytes 98304 | tf_op jit(solution)/shard_map/all_to_all | solution.py:23
  116.4 19.6 %all_to_all.46 = bf16[8,24,1024]{2,1,0:T(8,128)(2,1)S(1)} all-to-all(bf16[8,24,1024]{2,1,0:T(8,128)(2,1)S(1)} %broadcast_in_dim.22), channel_id=1, replica_groups=mesh['fs_0'=12,'fs_1'=8,'tp'=8] {'fs_1'}, dimensions={0} | all-to-all | bytes 786432 | tf_op jit(solution)/shard_map/all_to_all | solution.py:23
  136.0 0.1 multiply_reduce_fusion
  136.1 0.6 broadcast_in_dim.23
  136.7 4.9 %all-to-all-start.7 = ((f32[8,8,128]{2,1,0:T(8,128)}), f32[8,8,128]{2,1,0:T(8,128)S(1)}, u32[]{:S(2)}, u32[]{:S(2)}) async-start(f32[8,8,128]{2,1,0:T(8,128)} %broadcast_in_dim.23), calls=%async_computation.7 | async-start | bytes 65536 | tf_op jit(solution)/shard_map/all_to_all | solution.py:23
  141.6 0.2 copy.37
  141.8 0.4 copy.38
  142.3 0.9 reshape.64.dirs_ref
  143.2 1.8 %all-to-all-done.7.sums_ref = f32[8,8,128]{2,1,0:T(8,128)S(1)} async-done(((f32[8,8,128]{2,1,0:T(8,128)}), f32[8,8,128]{2,1,0:T(8,128)S(1)}, u32[]{:S(2)}, u32[]{:S(2)}) %all-to-all-start.7) | async-done | bytes 32800 | tf_op jit(solution)/shard_map/all_to_all | solution.py:23
  145.0 12.0 %all-gather.2.cloned.1.call-done.early_ref = bf16[2304,1408]{1,0:T(8,128)(2,1)} async-done(((bf16[24,1408]{1,0:T(8,128)(2,1)}), bf16[2304,1408]{1,0:T(8,128)(2,1)}) %all-gather.2.cloned.1.call-update) | async-done | bytes 6488080 | tf_op jit(solution)/shard_map/all_gather | solution.py:140
  156.9 6.7 %fold.1 = (bf16[2304,512]{1,0:T(8,128)(2,1)}, bf16[512,2304]{1,0:T(8,128)(2,1)}, f32[24,512]{1,0:T(8,128)}, f32[24,512]{1,0:T(8,128)}) custom-call(f32[8,8,128]{2,1,0:T(8,128)} %copy-done.3, bf16[2304,1408]{1,0:T(8,128)(2,1)} %all-gather.2.cloned.1.call-done.early_ref, bf16[24,192]{1,0:T(8,128)(2,1)} %own_value_ref.1, bf16[24,192]{1,0:T(8,128)(2,1)} %own_output_ref.1, ...), custom_call_target="tpu_custom_call" | custom-call | tf_op jit(solution)/shard_map/fold/pallas_call | solution.py:93
  (16 shorter events, 0.3 us)
Async XLA Ops:
  7.2 48.0 %copy-start = (bf16[512,2304]{1,0:T(8,128)(2,1)S(1)}, bf16[512,2304]{1,0:T(8,128)(2,1)}, u32[]{:S(2)}) copy-start(bf16[512,2304]{1,0:T(8,128)(2,1)} %param.15) | copy-start | bytes 7077892
  7.2 149.8 %all-gather.2.cloned.1.call-start = ((), (), s32[]{:S(2)}) async-start(), calls=%async_computation.8 | async-start | bytes 6555648 | tf_op jit(solution)/shard_map/all_gather | solution.py:140
  55.0 1.7 copy-start.1
  56.7 12.4 %copy-start.2 = (bf16[512,512]{1,0:T(8,128)(2,1)S(1)}, bf16[512,512]{1,0:T(8,128)(2,1)}, u32[]{:S(2)}) copy-start(bf16[512,512]{1,0:T(8,128)(2,1)} %param.13) | copy-start | bytes 1572868
  69.1 32.8 %copy-start.4 = (f32[2,512]{1,0:T(2,128)S(1)}, f32[2,512]{1,0:T(2,128)}, u32[]{:S(2)}) copy-start(f32[2,512]{1,0:T(2,128)} %param.21) | copy-start | bytes 12292
  69.1 32.8 %copy-start.5 = (f32[2,512]{1,0:T(2,128)S(1)}, f32[2,512]{1,0:T(2,128)}, u32[]{:S(2)}) copy-start(f32[2,512]{1,0:T(2,128)} %param.20) | copy-start | bytes 12292
  69.1 32.8 %copy-start.6 = (f32[2,512]{1,0:T(2,128)S(1)}, f32[2,512]{1,0:T(2,128)}, u32[]{:S(2)}) copy-start(f32[2,512]{1,0:T(2,128)} %param.23) | copy-start | bytes 12292
  69.1 32.8 %copy-start.7 = (f32[2,512]{1,0:T(2,128)S(1)}, f32[2,512]{1,0:T(2,128)}, u32[]{:S(2)}) copy-start(f32[2,512]{1,0:T(2,128)} %param.22) | copy-start | bytes 12292
  136.7 8.3 %all-to-all-start.7 = ((f32[8,8,128]{2,1,0:T(8,128)}), f32[8,8,128]{2,1,0:T(8,128)S(1)}, u32[]{:S(2)}, u32[]{:S(2)}) async-start(f32[8,8,128]{2,1,0:T(8,128)} %broadcast_in_dim.23), calls=%async_computation.7 | async-start | bytes 65536 | tf_op jit(solution)/shard_map/all_to_all | solution.py:23
  145.0 12.0 %copy-start.3 = (f32[8,8,128]{2,1,0:T(8,128)}, f32[8,8,128]{2,1,0:T(8,128)S(1)}, u32[]{:S(2)}) copy-start(f32[8,8,128]{2,1,0:T(8,128)S(1)} %all-to-all-done.7.sums_ref) | copy-start | bytes 98308
Sparse Core Ops, SparseCore 0:
  12.2 144.6 all-gather.1

commit v9 on v8

--- a/solution.py
+++ b/solution.py
@@ -136,9 +136,6 @@
     columns = value_cot.shape[1]
     deep, high = lax.axis_size("fs_0"), lax.axis_size("fs_1")
 
-    piece = [w_value.astype(bf16), w_output.T.astype(bf16), proj_value, proj_output]
-    early = lax.all_gather(jnp.concatenate(piece, axis=1), FS, axis=0, tiled=True)
-
     width = rank // lax.axis_size("tp")
     offset = lax.axis_index("tp") * width
     own = jnp.concatenate(
@@ -149,9 +146,13 @@
         axis=1,
     )
     share = spread(own.reshape(-1, proj_value.shape[0] * width), "fs_0")
-    share = spread(share.reshape(-1, proj_value.shape[0] * width), "fs_1")
-    rows = share.reshape(high, deep, -1, 2 * width)
+    share = share.reshape(-1, proj_value.shape[0] * width)
+    piece = [w_value.astype(bf16), w_output.T.astype(bf16), proj_value, proj_output, share]
+    near = spread(jnp.concatenate(piece, axis=1), "fs_1")
+    at = 2 * (columns + rank)
+    rows = near[:, :, at:].reshape(high, deep, -1, 2 * width)
     rows = jnp.swapaxes(rows, 0, 1).reshape(-1, 2 * width)
+    early = lax.all_gather(near[:, :, :at].reshape(-1, at), "fs_0", axis=0, tiled=True)
 
     narrow = jnp.concatenate(
         [

time: 171 us -> 169 us (0.988); the launches traced: 171 us -> 166 us
  blocking collectives: 118 us -> 99.5 us
  starting transfers between devices: 4.98 us -> 20.5 us
  waiting for transfers between devices: 13.8 us -> 10.7 us
    all_to_all x7 -> x6, blocking collectives: 118 us -> 99.5 us  [exchange(): return lax.all_to_all(pieces, axis, split_axis=0, concat_axis=0, tiled=True)]
    all_to_all x1 -> x2, starting transfers between devices: 4.94 us -> 20.5 us  [exchange(): return lax.all_to_all(pieces, axis, split_axis=0, concat_axis=0, tiled=True)]
    all_gather x1, waiting for transfers between devices: 12 us -> 0.01 us  [per_device(): lax.all_gather(near[:, :, :at].reshape(-1, at), 'fs_0', axis=0, tiled=True)]
    all_to_all x1 -> x2, waiting for transfers between devices: 1.81 us -> 10.7 us  [exchange(): return lax.all_to_all(pieces, axis, split_axis=0, concat_axis=0, tiled=True)]
  transfers between devices with their start and end apart: 2 -> 3, of which waited for: 2 -> 2; matrix products, arithmetic and copies ran while one was open for 5% -> 6% of each run, Pallas kernels for 0% -> 0%
where the time goes in v9:
time: 169 us; the launch traced here: 166 us
  blocking collectives  99.5 us (59%)
  starting transfers between devices  20.5 us (12%)
  between operations  14.3 us (8%)
  waiting for transfers between devices  10.7 us (6%)
  local copies, waits for them, and re-layouts  7.81 us (5%)
  Pallas kernels  6.74 us (4%)
  matrix products  3.39 us (2%)
  other arithmetic  2.58 us (2%)
    all_to_all x6, blocking collectives, exchange(): return lax.all_to_all(pieces, axis, split_axis=0, concat_axis=0, tiled=True)  99.5 us
    all_to_all x2, starting transfers between devices, exchange(): return lax.all_to_all(pieces, axis, split_axis=0, concat_axis=0, tiled=True)  20.5 us
    all_to_all x2, waiting for transfers between devices, exchange(): return lax.all_to_all(pieces, axis, split_axis=0, concat_axis=0, tiled=True)  10.7 us
    pallas_call x1, Pallas kernels, fold(): pl.pallas_call(functools.partial(fold_kernel, RANK * HV), grid=(rows // t...  6.74 us
    dot_general x4, matrix products, contract(): lax.dot_general(left, right, (dims, ((), ())), preferred_element_type=jnp...  3.39 us
  transfers between devices with their start and end apart: 3, of which 2 were waited for; matrix products, arithmetic and copies ran while one was open for 6% of the time, Pallas kernels for 0%

profile of v9, /device:TPU:6, one launch (start us, length us, event | category | flops | bytes accessed | tf_op | source)
XLA Modules:
  0.0 165.5 jit_solution(6332326662184715565)
XLA Ops:
  7.2 0.0 copy-start
  7.2 0.9 constant_dynamic-slice_fusion
  8.1 0.1 pad_maximum_fusion.2
  8.2 0.1 reshape.58
  8.3 0.6 broadcast_in_dim.18
  8.9 15.2 %all-to-all-start = ((bf16[12,2,576]{2,1,0:T(2,128)(2,1)}), bf16[12,2,576]{2,1,0:T(2,128)(2,1)S(1)}, u32[]{:S(2)}, u32[]{:S(2)}) async-start(bf16[12,2,576]{2,1,0:T(2,128)(2,1)} %broadcast_in_dim.18), calls=%async_computation | async-start | bytes 61440 | tf_op jit(solution)/shard_map/all_to_all | solution.py:23
  24.1 0.0 all-gather.2.cloned.1.call-start
  24.1 0.8 convert_bitcast_fusion
  25.0 0.8 convert_element_type.26
  25.8 8.9 %all-to-all-done = bf16[12,2,576]{2,1,0:T(2,128)(2,1)S(1)} async-done(((bf16[12,2,576]{2,1,0:T(2,128)(2,1)}), bf16[12,2,576]{2,1,0:T(2,128)(2,1)S(1)}, u32[]{:S(2)}, u32[]{:S(2)}) %all-to-all-start) | async-done | bytes 27680 | tf_op jit(solution)/shard_map/all_to_all | solution.py:23
  34.7 0.8 concatenate.19
  35.5 0.1 broadcast_in_dim.19
  35.6 28.6 %all_to_all.40 = bf16[8,24,1984]{2,1,0:T(8,128)(2,1)S(1)} all-to-all(bf16[8,24,1984]{2,1,0:T(8,128)(2,1)S(1)} %broadcast_in_dim.19), channel_id=1, replica_groups=mesh['fs_0'=12,'fs_1'=8,'tp'=8] {'fs_1'}, dimensions={0} | all-to-all | bytes 1523712 | tf_op jit(solution)/shard_map/all_to_all | solution.py:23
  64.1 0.8 slice.39
  65.0 0.0 all-gather.2.cloned.1.call-update
  65.1 0.5 reshape.60
  65.5 0.0 copy-start.1
  65.5 0.1 copy.33
  65.6 0.0 copy-done
  65.6 1.1 convolution_convert_fusion.2
  66.7 0.5 copy-done.1
  67.2 0.7 convolution_convert_fusion.3
  68.0 11.4 %all_to_all.41 = bf16[8,48,512]{2,1,0:T(8,128)(2,1)S(1)} all-to-all(bf16[8,48,512]{2,1,0:T(8,128)(2,1)S(1)} %broadcast_in_dim.20), channel_id=1, replica_groups=mesh['fs_0'=12,'fs_1'=8,'tp'=8] {'tp'}, dimensions={0} | all-to-all | bytes 786432 | tf_op jit(solution)/shard_map/all_to_all | solution.py:23
  79.4 0.1 dot_general.18
  79.5 0.1 dot_general.20
  79.6 0.0 copy-start.4
  79.6 0.0 copy-start.5
  79.6 0.0 copy-start.6
  79.7 0.0 copy-start.7
  79.7 0.3 convolution_convert_fusion.1
  79.9 1.3 convolution_convert_fusion
  81.3 0.2 copy.36
  81.5 17.2 %all_to_all.42 = bf16[8,24,1024]{2,1,0:T(8,128)(2,1)S(1)} all-to-all(bf16[8,24,1024]{2,1,0:T(8,128)(2,1)S(1)} %copy.36), channel_id=1, replica_groups=mesh['fs_0'=12,'fs_1'=8,'tp'=8] {'fs_1'}, dimensions={0} | all-to-all | bytes 786432 | tf_op jit(solution)/shard_map/all_to_all | solution.py:23
  98.7 0.1 reduce_sum.30
  98.8 14.0 %all_to_all.43 = bf16[12,2,1024]{2,1,0:T(2,128)(2,1)S(1)} all-to-all(bf16[12,2,1024]{2,1,0:T(2,128)(2,1)S(1)} %reshape.63), channel_id=1, replica_groups=mesh['fs_0'=12,'fs_1'=8,'tp'=8] {'fs_0'}, dimensions={0} | all-to-all | bytes 98304 | tf_op jit(solution)/shard_map/all_to_all | solution.py:23
  112.8 0.1 convert_reduce_fusion
  112.9 0.6 fusion.8
  113.6 14.0 %all_to_all.44 = bf16[12,2,1024]{2,1,0:T(2,128)(2,1)S(1)} all-to-all(bf16[12,2,1024]{2,1,0:T(2,128)(2,1)S(1)} %broadcast_in_dim.21), channel_id=1, replica_groups=mesh['fs_0'=12,'fs_1'=8,'tp'=8] {'fs_0'}, dimensions={0} | all-to-all | bytes 98304 | tf_op jit(solution)/shard_map/all_to_all | solution.py:23
  127.7 14.3 %all_to_all.45 = bf16[8,24,1024]{2,1,0:T(8,128)(2,1)S(1)} all-to-all(bf16[8,24,1024]{2,1,0:T(8,128)(2,1)S(1)} %broadcast_in_dim.22), channel_id=1, replica_groups=mesh['fs_0'=12,'fs_1'=8,'tp'=8] {'fs_1'}, dimensions={0} | all-to-all | bytes 786432 | tf_op jit(solution)/shard_map/all_to_all | solution.py:23
  141.9 0.1 multiply_reduce_fusion
  142.0 0.6 broadcast_in_dim.23
  142.6 5.3 %all-to-all-start.7 = ((f32[8,8,128]{2,1,0:T(8,128)}), f32[8,8,128]{2,1,0:T(8,128)S(1)}, u32[]{:S(2)}, u32[]{:S(2)}) async-start(f32[8,8,128]{2,1,0:T(8,128)} %broadcast_in_dim.23), calls=%async_computation.7 | async-start | bytes 65536 | tf_op jit(solution)/shard_map/all_to_all | solution.py:23
  148.0 0.2 copy.37
  148.2 0.4 copy.38
  148.6 0.9 reshape.68.dirs_ref
  149.5 1.8 %all-to-all-done.7.sums_ref = f32[8,8,128]{2,1,0:T(8,128)S(1)} async-done(((f32[8,8,128]{2,1,0:T(8,128)}), f32[8,8,128]{2,1,0:T(8,128)S(1)}, u32[]{:S(2)}, u32[]{:S(2)}) %all-to-all-start.7) | async-done | bytes 32800 | tf_op jit(solution)/shard_map/all_to_all | solution.py:23
  151.3 0.6 copy-done.3
  152.0 6.7 %fold.1 = (bf16[2304,512]{1,0:T(8,128)(2,1)}, bf16[512,2304]{1,0:T(8,128)(2,1)}, f32[24,512]{1,0:T(8,128)}, f32[24,512]{1,0:T(8,128)}) custom-call(f32[8,8,128]{2,1,0:T(8,128)} %copy-done.3, bf16[2304,1408]{1,0:T(8,128)(2,1)} %all-gather.2.cloned.1.call-done.early_ref, bf16[24,192]{1,0:T(8,128)(2,1)} %own_value_ref.1, bf16[24,192]{1,0:T(8,128)(2,1)} %own_output_ref.1, ...), custom_call_target="tpu_custom_call" | custom-call | tf_op jit(solution)/shard_map/fold/pallas_call | solution.py:93
  (19 shorter events, 0.3 us)
Async XLA Ops:
  7.2 58.5 %copy-start = (bf16[512,2304]{1,0:T(8,128)(2,1)S(1)}, bf16[512,2304]{1,0:T(8,128)(2,1)}, u32[]{:S(2)}) copy-start(bf16[512,2304]{1,0:T(8,128)(2,1)} %param.15) | copy-start | bytes 7077892
  8.9 25.7 %all-to-all-start = ((bf16[12,2,576]{2,1,0:T(2,128)(2,1)}), bf16[12,2,576]{2,1,0:T(2,128)(2,1)S(1)}, u32[]{:S(2)}, u32[]{:S(2)}) async-start(bf16[12,2,576]{2,1,0:T(2,128)(2,1)} %broadcast_in_dim.18), calls=%async_computation | async-start | bytes 61440 | tf_op jit(solution)/shard_map/all_to_all | solution.py:23
  24.1 127.2 %all-gather.2.cloned.1.call-start = ((), (), s32[]{:S(2)}) async-start(), calls=%async_computation.8 | async-start | bytes 7028736 | tf_op jit(solution)/shard_map/all_gather | solution.py:155
  65.5 1.7 %copy-start.1 = (bf16[512,2304]{1,0:T(8,128)(2,1)S(1)}, bf16[512,2304]{1,0:T(8,128)(2,1)}, u32[]{:S(2)}) copy-start(bf16[512,2304]{1,0:T(8,128)(2,1)} %param.12) | copy-start | bytes 7077892
  67.2 12.4 %copy-start.2 = (bf16[512,512]{1,0:T(8,128)(2,1)S(1)}, bf16[512,512]{1,0:T(8,128)(2,1)}, u32[]{:S(2)}) copy-start(bf16[512,512]{1,0:T(8,128)(2,1)} %param.13) | copy-start | bytes 1572868
  79.6 33.3 %copy-start.4 = (f32[2,512]{1,0:T(2,128)S(1)}, f32[2,512]{1,0:T(2,128)}, u32[]{:S(2)}) copy-start(f32[2,512]{1,0:T(2,128)} %param.21) | copy-start | bytes 12292
  79.6 33.3 %copy-start.5 = (f32[2,512]{1,0:T(2,128)S(1)}, f32[2,512]{1,0:T(2,128)}, u32[]{:S(2)}) copy-start(f32[2,512]{1,0:T(2,128)} %param.20) | copy-start | bytes 12292
  79.6 33.2 %copy-start.6 = (f32[2,512]{1,0:T(2,128)S(1)}, f32[2,512]{1,0:T(2,128)}, u32[]{:S(2)}) copy-start(f32[2,512]{1,0:T(2,128)} %param.23) | copy-start | bytes 12292
  79.7 33.2 %copy-start.7 = (f32[2,512]{1,0:T(2,128)S(1)}, f32[2,512]{1,0:T(2,128)}, u32[]{:S(2)}) copy-start(f32[2,512]{1,0:T(2,128)} %param.22) | copy-start | bytes 12292
  142.6 8.7 %all-to-all-start.7 = ((f32[8,8,128]{2,1,0:T(8,128)}), f32[8,8,128]{2,1,0:T(8,128)S(1)}, u32[]{:S(2)}, u32[]{:S(2)}) async-start(f32[8,8,128]{2,1,0:T(8,128)} %broadcast_in_dim.23), calls=%async_computation.7 | async-start | bytes 65536 | tf_op jit(solution)/shard_map/all_to_all | solution.py:23
  151.3 0.6 copy-start.3
Sparse Core Ops, SparseCore 0:
  65.1 78.5 all-gather.1
